TPU v7x, 512 devices: a whole 4x4x16 slice. The times are simulated.
512 devices in a mesh: ep: 32 (over z, core), tp: 16 (over y, x).
Axes of the slice: x: 4, y: 4, z: 16, core: 2. Of those that a mesh axis runs over, the one named last changes fastest.
Arguments:
- query_input: bfloat16 [16384, 2048], P('ep', 'tp'), may hold values from -6 to 6
- key_input: bfloat16 [16384, 1024], P('ep', 'tp'), may hold values from -6 to 6
- value_input: bfloat16 [16384, 1024], P('ep', 'tp'), may hold values from -64 to 64
- query_gain: float32 [64], replicated, may hold values from 0.5 to 6
- key_gain: float32 [64], replicated, may hold values from 0.5 to 6
- mixer_out: bfloat16 [2048, 4096], P(None, 'tp'), may hold values from -0.125 to 0.125
- moe_input: bfloat16 [8192, 4096], P('ep'), may hold values from -6 to 6
- moe_gain: float32 [4096], replicated, may hold values from 0.1 to 1.9
- routes: int32 [8192, 2], P('ep'), may hold values from 0 to 31, all different within a row; in each aligned block of 256 rows (0 to 255, 256 to 511, ...) at most 24 rows name the same one
- route_weight: float32 [8192, 2], P('ep'), may hold values from 0.1 to 1
- expert_gate: bfloat16 [32, 4096, 1024], P('ep', None, 'tp'), may hold values from -0.09375 to 0.09375
- expert_up: bfloat16 [32, 4096, 1024], P('ep', None, 'tp'), may hold values from -0.09375 to 0.09375
- expert_down: bfloat16 [32, 1024, 4096], P('ep', None, 'tp'), may hold values from -0.1875 to 0.1875
Outputs:
- attn_mixed: bfloat16 [16384, 4096], P('ep', 'tp')
- moe_out: bfloat16 [8192, 4096], P('ep', 'tp')
Inputs may be any that keep to these rules, and one draw needn't show every extreme that they name: `routes`: each row names 2 different experts. In the rows of one index of ep (aligned blocks of 256 rows) no expert is named by more than 24 rows, and in every draw some block has an expert named by exactly 24 rows.
All inputs are finite; a program needn't handle non-finite values.
Results may differ from a plain program's by a relative error of at most 0.0095.
The roundings to bfloat16 on the way count: a program that leaves them out, or rounds other values in their place, can miss the bound.
Values may be sent and summed in bfloat16 or wider, within the bound.
A program may use at most 64 MiB of HBM per device.

v0:
```python
import math

import jax
import jax.numpy as jnp
from jax import lax
from jax.sharding import Mesh
from jax.sharding import PartitionSpec as P

GRID_W = 64
TP = ("tp_0", "tp_1")


epsilon = 1e-06
base_theta = 10000.0


def gather_axes(x, axes, dim):
    for axis in reversed(axes):
        x = lax.all_gather(x, axis, axis=dim, tiled=True)
    return x


def copy_for_each(x, axis):
    copies = jnp.broadcast_to(x, (lax.axis_size(axis), *x.shape))
    return lax.all_to_all(copies, axis, split_axis=0, concat_axis=0, tiled=True)


def joined_along(parts, dim):
    parts = jnp.moveaxis(parts, 0, dim)
    shape = parts.shape
    return parts.reshape(*shape[:dim], shape[dim] * shape[dim + 1], *shape[dim + 2 :])


def gathered_copies(x, axis, dim):
    parts = copy_for_each(x, axis)
    return joined_along(parts, dim)


def rope_tables(positions, head_width):
    quarter = head_width // 4
    inverse = base_theta ** (-jnp.arange(quarter, dtype=jnp.float32) / quarter)
    grid_row = (positions // GRID_W).astype(jnp.float32)
    grid_col = (positions % GRID_W).astype(jnp.float32)
    angles = jnp.concatenate(
        [grid_row[:, None] * inverse[None, :], grid_col[:, None] * inverse[None, :]], axis=1
    )
    return (jnp.cos(angles), jnp.sin(angles))


def head_norm(heads_in, gain):
    return (
        heads_in * lax.rsqrt(jnp.mean(heads_in * heads_in, axis=-1, keepdims=True) + epsilon) * gain
    )


def rotate(heads_in, cosine, sine_table):
    half_width = heads_in.shape[-1] // 2
    first_half = heads_in[..., :half_width]
    second_half = heads_in[..., half_width:]
    cos_rows = cosine[:, None, :]
    sin_rows = sine_table[:, None, :]
    return jnp.concatenate(
        [
            first_half * cos_rows - second_half * sin_rows,
            first_half * sin_rows + second_half * cos_rows,
        ],
        axis=-1,
    )


def slot_places(route_block, expert_count, capacity):
    flat_routes = route_block.reshape(-1)
    one_hot = (flat_routes[:, None] == jnp.arange(expert_count, dtype=jnp.int32)[None, :]).astype(
        jnp.int32
    )
    earlier = jnp.cumsum(one_hot, axis=0) - one_hot
    return flat_routes * capacity + jnp.sum(earlier * one_hot, axis=1)


def fill_sources(places, token_count, top_count, slot_total):
    source_rows = jnp.full((slot_total,), token_count, jnp.int32)
    pair_rows = jnp.arange(token_count * top_count, dtype=jnp.int32) // top_count
    return source_rows.at[places].set(pair_rows)


def on_device(
    query_input,
    key_input,
    value_input,
    query_gain,
    key_gain,
    mixer_out,
    moe_input,
    moe_gain,
    routes,
    route_weight,
    expert_gate,
    expert_up,
    expert_down,
):
    seq_dev = query_input.shape[0]
    head_width = query_gain.shape[0]
    heads_here = query_input.shape[1] // head_width
    key_heads_here = key_input.shape[1] // head_width
    group_size = heads_here // key_heads_here
    positions = lax.axis_index("ep") * seq_dev + jnp.arange(seq_dev, dtype=jnp.int32)
    cosine, sine_table = rope_tables(positions, head_width)
    query_heads = query_input.astype(jnp.float32).reshape(seq_dev, heads_here, head_width)
    key_heads = key_input.astype(jnp.float32).reshape(seq_dev, key_heads_here, head_width)
    query_rot = rotate(head_norm(query_heads, query_gain), cosine, sine_table).astype(jnp.bfloat16)
    query_rot = query_rot.reshape(seq_dev, key_heads_here, group_size, head_width)
    key_rot = rotate(head_norm(key_heads, key_gain), cosine, sine_table).astype(jnp.bfloat16)
    key_value = jnp.concatenate(
        [key_rot.reshape(seq_dev, key_heads_here * head_width), value_input], axis=1
    )
    score_scale = head_width ** (-0.5)
    initial = (
        jnp.full((key_heads_here, group_size, seq_dev), -jnp.inf, jnp.float32),
        jnp.zeros((key_heads_here, group_size, seq_dev), jnp.float32),
        jnp.zeros((seq_dev, key_heads_here, group_size, head_width), jnp.float32),
    )
    incoming = lax.all_gather(key_value, "ep", axis=0, tiled=True)
    incoming_rows = incoming.shape[0]
    block_len = math.gcd(incoming_rows, 512)
    key_blocks = incoming.reshape(
        incoming_rows // block_len, block_len, 2, key_heads_here, head_width
    )

    def one_block(current, key_block):
        largest, denominator, numerator = current
        scores = (
            jnp.einsum(
                "qkgd,skd->kgqs", query_rot, key_block[:, 0], preferred_element_type=jnp.float32
            )
            * score_scale
        )
        new_largest = jnp.maximum(largest, jnp.max(scores, axis=-1))
        weights = jnp.exp(scores - new_largest[..., None])
        factor = jnp.exp(largest - new_largest)
        denominator = denominator * factor + jnp.sum(weights, axis=-1)
        contribution = jnp.einsum(
            "kgqs,skd->qkgd",
            weights.astype(jnp.bfloat16),
            key_block[:, 1],
            preferred_element_type=jnp.float32,
        )
        numerator = numerator * jnp.transpose(factor, (2, 0, 1))[..., None] + contribution
        return ((new_largest, denominator, numerator), None)

    current, _ = lax.scan(one_block, initial, key_blocks)
    largest, denominator, numerator = current
    attended = numerator / jnp.transpose(denominator, (2, 0, 1))[..., None]
    attended = attended.reshape(seq_dev, heads_here * head_width).astype(jnp.bfloat16)
    projected = jnp.dot(gather_axes(attended, TP, 1), mixer_out, preferred_element_type=jnp.float32)
    attn_mixed = projected.astype(jnp.bfloat16)
    token_count, model_width = moe_input.shape
    top_count = routes.shape[1]
    local_experts = expert_gate.shape[0]
    senders = lax.axis_size("ep")
    expert_count = local_experts * senders
    capacity = 3 * token_count * top_count // (2 * expert_count)
    features = moe_input.astype(jnp.float32)
    normed = (
        features
        * lax.rsqrt(jnp.mean(features * features, axis=-1, keepdims=True) + epsilon)
        * moe_gain
    ).astype(jnp.bfloat16)
    places = slot_places(routes, expert_count, capacity)
    sources = fill_sources(places, token_count, top_count, expert_count * capacity)
    padded = jnp.concatenate([normed, jnp.zeros((1, model_width), jnp.bfloat16)], axis=0)
    column_width = expert_down.shape[2]
    feature_width = model_width // lax.axis_size(TP)
    own_columns = lax.dynamic_slice_in_dim(
        padded, lax.axis_index(TP) * feature_width, feature_width, 1
    )
    received = lax.all_to_all(own_columns[sources], "ep", split_axis=0, concat_axis=0, tiled=True)
    received = received.reshape(senders, local_experts, capacity, feature_width)
    incoming = lax.all_gather(received, TP, axis=3, tiled=True)
    gate_hidden = jnp.einsum(
        "sjcd,jdf->sjcf", incoming, expert_gate, preferred_element_type=jnp.float32
    )
    up_hidden = jnp.einsum(
        "sjcd,jdf->sjcf", incoming, expert_up, preferred_element_type=jnp.float32
    )
    hidden = (jax.nn.silu(gate_hidden) * up_hidden).astype(jnp.bfloat16)
    expert_out = jnp.einsum(
        "sjcf,jfd->sjcd",
        gathered_copies(hidden, TP, 3),
        expert_down,
        preferred_element_type=jnp.float32,
    )
    expert_out = expert_out.astype(jnp.bfloat16).reshape(
        senders * local_experts * capacity, column_width
    )
    returned = lax.all_to_all(expert_out, "ep", split_axis=0, concat_axis=0, tiled=True)
    picked = returned[places].reshape(token_count, top_count, column_width).astype(jnp.float32)
    shares = route_weight / jnp.sum(route_weight, axis=-1, keepdims=True)
    moe_out = jnp.sum(picked * shares[:, :, None], axis=1).astype(jnp.bfloat16)
    return (attn_mixed, moe_out)


def solution(mesh):
    torus = Mesh(mesh.devices.reshape(mesh.shape["ep"], 4, 4), ("ep", "tp_0", "tp_1"))
    placed = (
        P("ep", TP),
        P("ep", TP),
        P("ep", TP),
        P(),
        P(),
        P(None, TP),
        P("ep", None),
        P(),
        P("ep", None),
        P("ep", None),
        P("ep", None, TP),
        P("ep", None, TP),
        P("ep", None, TP),
    )
    return jax.shard_map(
        on_device,
        mesh=torus,
        in_specs=placed,
        out_specs=(P("ep", TP), P("ep", TP)),
        check_vma=False,
    )
```

profile of v0, /device:TPU:1, one launch (start us, length us, event | category | flops | bytes accessed | tf_op | source)
XLA Modules:
  0.0 329.3 jit_solution(3318978957161452941)
XLA Ops:
  9.6 1.5 pad_maximum_fusion
  14.8 2.4 scatter_custom_fusion
  18.6 3.3 gather_fusion
  21.9 16.7 %all-to-all-start = ((bf16[32,24,256]{2,1,0:T(8,128)(2,1)}), bf16[32,24,256]{2,1,0:T(8,128)(2,1)S(1)}, u32[]{:S(2)}, u32[]{:S(2)}) async-start(bf16[32,24,256]{2,1,0:T(8,128)(2,1)} %bitcast.14), calls=%async_computation | async-start | bytes 786432 | tf_op jit(solution)/shard_map/all_to_all | solution.py:176
  40.1 30.2 %all-to-all-done = bf16[32,24,256]{2,1,0:T(8,128)(2,1)S(1)} async-done(((bf16[32,24,256]{2,1,0:T(8,128)(2,1)}), bf16[32,24,256]{2,1,0:T(8,128)(2,1)S(1)}, u32[]{:S(2)}, u32[]{:S(2)}) %all-to-all-start) | async-done | bytes 393248 | tf_op jit(solution)/shard_map/all_to_all | solution.py:176
  71.2 30.8 %all-gather.5.cloned.1.call-done = bf16[16384,128]{0,1:T(8,128)(2,1)} async-done(((bf16[512,128]{0,1:T(8,128)(2,1)}), bf16[16384,128]{0,1:T(8,128)(2,1)}) %all-gather.5.cloned.1.call-update) | async-done | bytes 4194320 | tf_op jit(solution)/shard_map/all_gather | solution.py:122
  102.0 3.9 %copy.37 = bf16[16,8,32,512]{3,2,1,0:T(8,128)(2,1)S(1)} copy(bf16[16,8,32,512]{3,1,2,0:T(8,128)(2,1)} %bitcast.174) | data formatting | bytes 8388608
  105.9 4.4 %copy.28 = bf16[32,512,2,1,64]{1,4,2,3,0:T(8,128)(2,1)} copy(bf16[32,512,2,1,64]{1,0,4,2,3:T(8,128)(2,1)S(1)} %bitcast.172) | data formatting | bytes 8388608
  110.3 104.1 %while.15 = (s32[]{:T(128)}, f32[1,2,512]{2,1,0:T(2,128)S(1)}, f32[1,2,512]{2,1,0:T(2,128)S(1)}, f32[512,1,2,64]{0,3,2,1:T(8,128)S(1)}, bf16[32,512,2,1,64]{1,4,...) while((s32[]{:T(128)}, f32[1,2,512]{2,1,0:T(2,128)S(1)}, ...), condition=%wide.region_5.6_spmd.clone, body=%wide.region_2.5_spmd.clone.sunk | while | flops 138614784 | bytes 7405669 | solution.py:150
  114.5 1.4 bitcast_reduce_fusion.2
  117.8 1.4 bitcast_reduce_fusion.2
  121.0 1.4 bitcast_reduce_fusion.2
  124.3 1.4 bitcast_reduce_fusion.2
  127.5 1.4 bitcast_reduce_fusion.2
  130.8 1.4 bitcast_reduce_fusion.2
  137.3 1.4 bitcast_reduce_fusion.2
  140.5 1.4 bitcast_reduce_fusion.2
  143.8 1.4 bitcast_reduce_fusion.2
  147.0 1.4 bitcast_reduce_fusion.2
  150.3 1.4 bitcast_reduce_fusion.2
  156.8 1.4 bitcast_reduce_fusion.2
  160.1 1.4 bitcast_reduce_fusion.2
  163.3 1.4 bitcast_reduce_fusion.2
  166.6 1.4 bitcast_reduce_fusion.2
  169.8 1.4 bitcast_reduce_fusion.2
  173.1 1.4 bitcast_reduce_fusion.2
  176.4 1.4 bitcast_reduce_fusion.2
  179.6 1.4 bitcast_reduce_fusion.2
  182.9 1.4 bitcast_reduce_fusion.2
  186.1 1.4 bitcast_reduce_fusion.2
  195.9 1.4 bitcast_reduce_fusion.2
  208.9 1.4 bitcast_reduce_fusion.2
  214.5 4.8 %convolution_bitcast_fusion.2 = f32[32,1,24,64]{3,2,0,1:T(8,128)S(1)} fusion(bf16[32,24,4096]{2,1,0:T(8,128)(2,1)} %all-gather.9.cloned.1.call-done, bf16[1,4096,64]{1,2,0:T(8,128)(2,1)} %param.25), kind=kOutput, calls=%fused_computation.35 | convolution fusion | flops 402653184 | bytes 7012352 | tf_op jit(solution)/shard_map/sjcd,jdf->sjcf/dot_general | solution.py:179
  219.4 1.9 fusion.17
  221.3 2.3 broadcast_bitcast_fusion
  223.6 4.9 %reshape.442 = bf16[16,2,24576]{2,1,0:T(2,128)(2,1)} reshape(bf16[16,1,32,24,64]{4,3,2,1,0:T(8,128)(2,1)} %broadcast_bitcast_fusion) | data formatting | bytes 3145728
  228.5 6.3 %all-to-all-start.1 = ((bf16[16,2,24576]{2,1,0:T(2,128)(2,1)}), bf16[16,2,24576]{2,1,0:T(2,128)(2,1)S(1)}, u32[]{:S(2)}, u32[]{:S(2)}) async-start(bf16[16,2,24576]{2,1,0:T(2,128)(2,1)} %reshape.442), calls=%async_computation.1 | async-start | bytes 3145728 | tf_op jit(solution)/shard_map/all_to_all | solution.py:25
  235.0 29.6 %all_gather.13 = bf16[512,512]{0,1:T(8,128)(2,1)} all-gather(bf16[512,128]{0,1:T(8,128)(2,1)S(1)} %bitcast.177), channel_id=1, replica_groups=mesh['ep'=32,'tp_0'=4,'tp_1'=4] {'tp_1'}, dimensions={1}, use_global_device_ids=true | all-gather | bytes 655360 | tf_op jit(solution)/shard_map/all_gather | solution.py:19
  264.6 3.3 %reshape.443 = bf16[16,1,32,24,64]{4,3,2,1,0:T(8,128)(2,1)} reshape(bf16[16,2,24576]{2,1,0:T(2,128)(2,1)S(1)} %all-to-all-done.1) | data formatting | bytes 3145728
  268.0 2.6 bitcast_bitcast_fusion.1
  270.5 5.3 %copy.33 = bf16[32,1,24,16,64]{4,3,2,0,1:T(8,128)(2,1)} copy(bf16[32,1,24,16,64]{4,2,0,1,3:T(8,128)(2,1)S(1)} %bitcast_bitcast_fusion.1) | data formatting | bytes 3145728 | tf_op jit(solution)/shard_map/transpose | solution.py:29
  275.8 4.6 %reshape.398 = bf16[32,24,1024]{2,1,0:T(8,128)(2,1)S(1)} reshape(bf16[32,1,24,16,64]{4,3,2,0,1:T(8,128)(2,1)} %copy.33) | data formatting | bytes 3145728 | tf_op jit(solution)/shard_map/reshape.35
  281.8 9.7 %all-to-all-start.2 = ((bf16[32,24,256]{2,1,0:T(8,128)(2,1)}), bf16[32,24,256]{2,1,0:T(8,128)(2,1)S(1)}, u32[]{:S(2)}, u32[]{:S(2)}) async-start(bf16[32,24,256]{2,1,0:T(8,128)(2,1)} %convolution_convert_fusion), calls=%async_computation.2 | async-start | bytes 786432 | tf_op jit(solution)/shard_map/all_to_all | solution.py:195
  291.6 8.6 %all-gather.7.cloned.1.call-done = bf16[512,2048]{0,1:T(8,128)(2,1)} async-done(((bf16[512,512]{0,1:T(8,128)(2,1)}), bf16[512,2048]{0,1:T(8,128)(2,1)}) %all-gather.7.cloned.1.call-update) | async-done | bytes 2097168 | tf_op jit(solution)/shard_map/all_gather | solution.py:19
  300.2 3.0 convolution_convert_fusion.1
  303.3 15.9 %all-to-all-done.2 = bf16[32,24,256]{2,1,0:T(8,128)(2,1)S(1)} async-done(((bf16[32,24,256]{2,1,0:T(8,128)(2,1)}), bf16[32,24,256]{2,1,0:T(8,128)(2,1)S(1)}, u32[]{:S(2)}, u32[]{:S(2)}) %all-to-all-start.2) | async-done | bytes 393248 | tf_op jit(solution)/shard_map/all_to_all | solution.py:195
  319.2 1.9 gather_fusion.1
  321.4 1.4 multiply_reduce_fusion
  (273 shorter events, 82.3 us)
Async XLA Ops:
  7.2 293.1 %copy-start = (bf16[2048,256]{1,0:T(8,128)(2,1)S(1)}, bf16[2048,256]{1,0:T(8,128)(2,1)}, u32[]{:S(2)}) copy-start(bf16[2048,256]{1,0:T(8,128)(2,1)} %param.20) | copy-start | bytes 3145732
  7.2 10.1 %copy-start.1 = (bf16[256,4096]{1,0:T(8,128)(2,1)S(1)}, bf16[256,4096]{1,0:T(8,128)(2,1)}, u32[]{:S(2)}) copy-start(bf16[256,4096]{1,0:T(8,128)(2,1)} %param.21) | copy-start | bytes 6291460
  7.2 94.8 %all-gather.5.cloned.1.call-start = ((), (), s32[]{:S(2)}) async-start(), calls=%async_computation.3 | async-start | bytes 4325376 | tf_op jit(solution)/shard_map/all_gather | solution.py:122
  8.3 9.5 %copy-start.4 = (f32[4096]{0:T(1024)S(1)}, f32[4096]{0:T(1024)}, u32[]{:S(2)}) copy-start(f32[4096]{0:T(1024)} %param.22) | copy-start | bytes 49156
  18.6 20.3 %copy-start.3 = (bf16[512,128]{1,0:T(8,128)(2,1)S(1)}, bf16[512,128]{1,0:T(8,128)(2,1)}, u32[]{:S(2)}) copy-start(bf16[512,128]{1,0:T(8,128)(2,1)} %param.15) | copy-start | bytes 393220
  18.6 20.7 %copy-start.6 = (f32[64]{0:T(128)S(1)}, f32[64]{0:T(128)}, u32[]{:S(2)}) copy-start(f32[64]{0:T(128)} %param.18) | copy-start | bytes 772
  21.9 48.5 %all-to-all-start = ((bf16[32,24,256]{2,1,0:T(8,128)(2,1)}), bf16[32,24,256]{2,1,0:T(8,128)(2,1)S(1)}, u32[]{:S(2)}, u32[]{:S(2)}) async-start(bf16[32,24,256]{2,1,0:T(8,128)(2,1)} %bitcast.14), calls=%async_computation | async-start | bytes 786432 | tf_op jit(solution)/shard_map/all_to_all | solution.py:176
  38.6 175.9 %all-gather.9.cloned.1.call-start = ((), (), s32[]{:S(2)}) async-start(), calls=%async_computation.5 | async-start | bytes 6684672 | tf_op jit(solution)/shard_map/all_gather | solution.py:178
  70.4 0.8 copy-start.2
  214.4 4.8 %copy-start.8 = (bf16[1,4096,64]{1,2,0:T(8,128)(2,1)S(1)}, bf16[1,4096,64]{1,2,0:T(8,128)(2,1)}, u32[]{:S(2)}) copy-start(bf16[1,4096,64]{1,2,0:T(8,128)(2,1)} %param.26) | copy-start | bytes 1572868
  214.5 4.9 %copy-start.7 = (bf16[32,24,4096]{2,1,0:T(8,128)(2,1)S(1)}, bf16[32,24,4096]{2,1,0:T(8,128)(2,1)}, u32[]{:S(2)}) copy-start(bf16[32,24,4096]{2,1,0:T(8,128)(2,1)} %all-gather.9.cloned.1.call-done) | copy-start | bytes 18874372
  228.5 36.1 %all-to-all-start.1 = ((bf16[16,2,24576]{2,1,0:T(2,128)(2,1)}), bf16[16,2,24576]{2,1,0:T(2,128)(2,1)S(1)}, u32[]{:S(2)}, u32[]{:S(2)}) async-start(bf16[16,2,24576]{2,1,0:T(2,128)(2,1)} %reshape.442), calls=%async_computation.1 | async-start | bytes 3145728 | tf_op jit(solution)/shard_map/all_to_all | solution.py:25
  234.9 65.3 %all-gather.7.cloned.1.call-start = ((), (), s32[]{:S(2)}) async-start(), calls=%async_computation.4 | async-start | bytes 2621440 | tf_op jit(solution)/shard_map/all_gather | solution.py:19
  275.8 4.6 %copy-start.9 = (bf16[1,1024,256]{2,1,0:T(8,128)(2,1)S(1)}, bf16[1,1024,256]{2,1,0:T(8,128)(2,1)}, u32[]{:S(2)}) copy-start(bf16[1,1024,256]{2,1,0:T(8,128)(2,1)} %param.27) | copy-start | bytes 1572868
  280.4 11.0 %copy-start.5 = (f32[256,2]{0,1:T(2,128)S(1)}, f32[256,2]{0,1:T(2,128)}, u32[]{:S(2)}) copy-start(f32[256,2]{0,1:T(2,128)} %param.24) | copy-start | bytes 6148
  281.8 37.4 %all-to-all-start.2 = ((bf16[32,24,256]{2,1,0:T(8,128)(2,1)}), bf16[32,24,256]{2,1,0:T(8,128)(2,1)S(1)}, u32[]{:S(2)}, u32[]{:S(2)}) async-start(bf16[32,24,256]{2,1,0:T(8,128)(2,1)} %convolution_convert_fusion), calls=%async_computation.2 | async-start | bytes 786432 | tf_op jit(solution)/shard_map/all_to_all | solution.py:195
Sparse Core Ops, SparseCore 0:
  11.2 90.6 all-gather.4
  105.0 76.9 all-gather.8
  264.7 35.4 all-gather.6
where the time goes:
time: 331 us; the launch traced here: 329 us
  waiting for transfers between devices  85.6 us (26%)
  local copies, waits for them, and re-layouts  71.6 us (22%)
  matrix products  71.3 us (22%)
  starting transfers between devices  33 us (10%)
  blocking collectives  29.6 us (9%)
  other arithmetic  22.3 us (7%)
  between operations  14.2 us (4%)
    dot_general x32, matrix products, one_block(): jnp.einsum('qkgd,skd->kgqs', query_rot, key_block[:, 0], preferred_elemen...  43.9 us
    all_gather x1, waiting for transfers between devices, on_device(): incoming = lax.all_gather(key_value, 'ep', axis=0, tiled=True)  30.8 us
    all_to_all x1, waiting for transfers between devices, on_device(): lax.all_to_all(own_columns[sources], 'ep', split_axis=0, concat_axis=0, t...  30.2 us
    all_gather x1, blocking collectives, gather_axes(): x = lax.all_gather(x, axis, axis=dim, tiled=True)  29.6 us
    squeeze x32, local copies, waits for them, and re-layouts, on_device(): current, _ = lax.scan(one_block, initial, key_blocks)  29.4 us
    unnamed x26, local copies, waits for them, and re-layouts  20.6 us
    all_to_all x1, starting transfers between devices, on_device(): lax.all_to_all(own_columns[sources], 'ep', split_axis=0, concat_axis=0, t...  16.7 us
    dot_general x32, matrix products, one_block(): jnp.einsum('kgqs,skd->qkgd', weights.astype(jnp.bfloat16), key_block[:, 1...  16.3 us
  transfers between devices with their start and end apart: 6, of which 4 were waited for; matrix products, arithmetic and copies ran while one was open for 43% of the time, Pallas kernels for 0%

commit v1 on v0

--- a/solution.py
+++ b/solution.py
@@ -1,8 +1,10 @@
-import math
+import functools
 
 import jax
 import jax.numpy as jnp
 from jax import lax
+from jax.experimental import pallas as pl
+from jax.experimental.pallas import tpu as pltpu
 from jax.sharding import Mesh
 from jax.sharding import PartitionSpec as P
 
@@ -42,30 +44,115 @@
     grid_row = (positions // GRID_W).astype(jnp.float32)
     grid_col = (positions % GRID_W).astype(jnp.float32)
     angles = jnp.concatenate(
-        [grid_row[:, None] * inverse[None, :], grid_col[:, None] * inverse[None, :]], axis=1
+        [inverse[:, None] * grid_row[None, :], inverse[:, None] * grid_col[None, :]], axis=0
     )
     return (jnp.cos(angles), jnp.sin(angles))
 
 
-def head_norm(heads_in, gain):
-    return (
-        heads_in * lax.rsqrt(jnp.mean(heads_in * heads_in, axis=-1, keepdims=True) + epsilon) * gain
-    )
-
-
-def rotate(heads_in, cosine, sine_table):
-    half_width = heads_in.shape[-1] // 2
-    first_half = heads_in[..., :half_width]
-    second_half = heads_in[..., half_width:]
-    cos_rows = cosine[:, None, :]
-    sin_rows = sine_table[:, None, :]
+def rotated(x, cosine, sine, gain):
+    scale = lax.rsqrt(jnp.mean(x * x, axis=0, keepdims=True) + epsilon)
+    x = x * scale * gain
+    half = x.shape[0] // 2
+    first, second = x[:half], x[half:]
     return jnp.concatenate(
-        [
-            first_half * cos_rows - second_half * sin_rows,
-            first_half * sin_rows + second_half * cos_rows,
+        [first * cosine - second * sine, first * sine + second * cosine], axis=0
+    )
+
+
+def key_value_kernel(width, k_ref, v_ref, cos_ref, sin_ref, gain_ref, out_ref):
+    k_t = k_ref[...].astype(jnp.float32).T
+    k_t = rotated(k_t, cos_ref[...], sin_ref[...], gain_ref[...])
+    v = v_ref[...].astype(jnp.float32)
+    out_ref[...] = jnp.concatenate([k_t.T, v], axis=1).astype(jnp.bfloat16)
+
+
+def flash_kernel(
+    width, block, q_ref, kv_ref, cos_ref, sin_ref, gain_ref, out_ref, qt_ref, s_ref, mx_ref, m_ref, o_ref
+):
+    rows = q_ref.shape[0]
+    heads = q_ref.shape[1] // width
+    lanes = heads * rows
+    blocks = kv_ref.shape[0] // block
+    q_t = q_ref[...].astype(jnp.float32).T
+    for head in range(heads):
+        turned = rotated(
+            q_t[head * width : (head + 1) * width], cos_ref[...], sin_ref[...], gain_ref[...]
+        )
+        turned = turned.astype(jnp.bfloat16).astype(jnp.float32) * (width ** (-0.5))
+        qt_ref[:width, head * rows : (head + 1) * rows] = turned.astype(jnp.bfloat16)
+    qt_ref[width:, :] = jnp.zeros((width, lanes), jnp.bfloat16)
+    m_ref[...] = jnp.full(m_ref.shape, -1e30, jnp.float32)
+    o_ref[...] = jnp.zeros(o_ref.shape, jnp.float32)
+    log2e = 1.4426950408889634
+
+    def scores(index, slot):
+        keys = kv_ref[pl.ds(pl.multiple_of(index * block, block), block), :]
+        s = jnp.dot(keys, qt_ref[...], preferred_element_type=jnp.float32)
+        s_ref[slot] = s
+        mx_ref[slot] = jnp.max(s.reshape(block // 8, 8, lanes), axis=0)
+
+    def absorb(index, slot):
+        old = m_ref[...]
+        new = jnp.maximum(old, jnp.max(mx_ref[slot], axis=0, keepdims=True) * log2e)
+        m_ref[...] = new
+        factor = jnp.exp2(old - new)
+        p = jnp.exp2(s_ref[slot] * log2e - new[:1]).astype(jnp.bfloat16)
+        kv = kv_ref[pl.ds(pl.multiple_of(index * block, block), block), :]
+        v_t = kv.T[width:]
+        lhs = jnp.concatenate([jnp.ones((16, block), jnp.bfloat16), v_t], axis=0)
+        part = jnp.dot(lhs, p, preferred_element_type=jnp.float32)
+        o_ref[...] = o_ref[...] * factor[:1] + part
+
+    scores(0, 0)
+
+    @pl.loop(0, blocks - 1)
+    def _(index):
+        slot = lax.rem(index, 2)
+        scores(index + 1, 1 - slot)
+        absorb(index, slot)
+
+    absorb(blocks - 1, (blocks - 1) % 2)
+    attended = o_ref[16:, :] / o_ref[:1, :]
+    for head in range(heads):
+        out_ref[:, head * width : (head + 1) * width] = (
+            attended[:, head * rows : (head + 1) * rows].T.astype(jnp.bfloat16)
+        )
+
+
+def vmem():
+    return pl.BlockSpec(memory_space=pltpu.VMEM)
+
+
+def key_value_rows(key_input, value_input, cosine, sine, gain):
+    rows, width = key_input.shape
+    return pl.pallas_call(
+        functools.partial(key_value_kernel, width),
+        out_shape=jax.ShapeDtypeStruct((rows, 2 * width), jnp.bfloat16),
+        in_specs=[vmem()] * 5,
+        out_specs=vmem(),
+    )(key_input, value_input, cosine, sine, gain)
+
+
+def flash(query_input, key_values, cosine, sine, gain):
+    rows, columns = query_input.shape
+    width = gain.shape[0]
+    lanes = rows * (columns // width)
+    block = 512
+    return pl.pallas_call(
+        functools.partial(flash_kernel, width, block),
+        out_shape=jax.ShapeDtypeStruct((rows, columns), jnp.bfloat16),
+        in_specs=[vmem()] * 5,
+        out_specs=vmem(),
+        scratch_shapes=[
+            pltpu.VMEM((2 * width, lanes), jnp.bfloat16),
+            pltpu.VMEM((2, block, lanes), jnp.float32),
+            pltpu.VMEM((2, 8, lanes), jnp.float32),
+            pltpu.VMEM((8, lanes), jnp.float32),
+            pltpu.VMEM((16 + width, lanes), jnp.float32),
         ],
-        axis=-1,
-    )
+        compiler_params=pltpu.CompilerParams(vmem_limit_bytes=40 * 1024 * 1024),
+        cost_estimate=pl.CostEstimate(flops=20_000_000_000, bytes_accessed=5_000_000, transcendentals=0),
+    )(query_input, key_values, cosine, sine, gain)
 
 
 def slot_places(route_block, expert_count, capacity):
@@ -100,57 +187,13 @@
 ):
     seq_dev = query_input.shape[0]
     head_width = query_gain.shape[0]
-    heads_here = query_input.shape[1] // head_width
-    key_heads_here = key_input.shape[1] // head_width
-    group_size = heads_here // key_heads_here
     positions = lax.axis_index("ep") * seq_dev + jnp.arange(seq_dev, dtype=jnp.int32)
     cosine, sine_table = rope_tables(positions, head_width)
-    query_heads = query_input.astype(jnp.float32).reshape(seq_dev, heads_here, head_width)
-    key_heads = key_input.astype(jnp.float32).reshape(seq_dev, key_heads_here, head_width)
-    query_rot = rotate(head_norm(query_heads, query_gain), cosine, sine_table).astype(jnp.bfloat16)
-    query_rot = query_rot.reshape(seq_dev, key_heads_here, group_size, head_width)
-    key_rot = rotate(head_norm(key_heads, key_gain), cosine, sine_table).astype(jnp.bfloat16)
-    key_value = jnp.concatenate(
-        [key_rot.reshape(seq_dev, key_heads_here * head_width), value_input], axis=1
-    )
-    score_scale = head_width ** (-0.5)
-    initial = (
-        jnp.full((key_heads_here, group_size, seq_dev), -jnp.inf, jnp.float32),
-        jnp.zeros((key_heads_here, group_size, seq_dev), jnp.float32),
-        jnp.zeros((seq_dev, key_heads_here, group_size, head_width), jnp.float32),
+    key_value = key_value_rows(
+        key_input, value_input, cosine, sine_table, key_gain[:, None]
     )
     incoming = lax.all_gather(key_value, "ep", axis=0, tiled=True)
-    incoming_rows = incoming.shape[0]
-    block_len = math.gcd(incoming_rows, 512)
-    key_blocks = incoming.reshape(
-        incoming_rows // block_len, block_len, 2, key_heads_here, head_width
-    )
-
-    def one_block(current, key_block):
-        largest, denominator, numerator = current
-        scores = (
-            jnp.einsum(
-                "qkgd,skd->kgqs", query_rot, key_block[:, 0], preferred_element_type=jnp.float32
-            )
-            * score_scale
-        )
-        new_largest = jnp.maximum(largest, jnp.max(scores, axis=-1))
-        weights = jnp.exp(scores - new_largest[..., None])
-        factor = jnp.exp(largest - new_largest)
-        denominator = denominator * factor + jnp.sum(weights, axis=-1)
-        contribution = jnp.einsum(
-            "kgqs,skd->qkgd",
-            weights.astype(jnp.bfloat16),
-            key_block[:, 1],
-            preferred_element_type=jnp.float32,
-        )
-        numerator = numerator * jnp.transpose(factor, (2, 0, 1))[..., None] + contribution
-        return ((new_largest, denominator, numerator), None)
-
-    current, _ = lax.scan(one_block, initial, key_blocks)
-    largest, denominator, numerator = current
-    attended = numerator / jnp.transpose(denominator, (2, 0, 1))[..., None]
-    attended = attended.reshape(seq_dev, heads_here * head_width).astype(jnp.bfloat16)
+    attended = flash(query_input, incoming, cosine, sine_table, query_gain[:, None])
     projected = jnp.dot(gather_axes(attended, TP, 1), mixer_out, preferred_element_type=jnp.float32)
     attn_mixed = projected.astype(jnp.bfloat16)
     token_count, model_width = moe_input.shape

time: 331 us -> 328 us (level)
  waiting for transfers between devices: 85.6 us -> 150 us
  matrix products: 71.3 us -> 11 us
  Pallas kernels: 0 us -> 35.5 us
  local copies, waits for them, and re-layouts: 71.6 us -> 36.9 us
  blocking collectives: 29.6 us -> 57.5 us
  starting transfers between devices: 33 us -> 15.2 us
  other arithmetic: 22.3 us -> 7.26 us
    all_gather x1, waiting for transfers between devices: 0.02 us -> 67.1 us  [on_device(): incoming = lax.all_gather(received, TP, axis=3, tiled=True)]
    dot_general x64 -> x0, matrix products: 60.2 us -> none  [the longest x32 43.9 us: one_block(): jnp.einsum('qkgd,skd->kgqs', query_rot, key_block[:, 0], preferred_elemen...]
    all_to_all x0 -> x1, blocking collectives: none -> 44.4 us  [on_device(): lax.all_to_all(own_columns[sources], 'ep', split_axis=0, concat_axis=0, t...]
    pallas_call x0 -> x2, Pallas kernels: none -> 35.5 us  [the longest x1 33.5 us: flash(): pl.pallas_call(functools.partial(flash_kernel, width, block), out_shape=j...]
    all_to_all x1 -> x0, waiting for transfers between devices: 30.2 us -> none  [on_device(): lax.all_to_all(own_columns[sources], 'ep', split_axis=0, concat_axis=0, t...]
    squeeze x32 -> x0, local copies, waits for them, and re-layouts: 29.4 us -> none  [on_device(): current, _ = lax.scan(one_block, initial, key_blocks)]
    all_gather x1, waiting for transfers between devices: 30.8 us -> 58 us  [on_device(): incoming = lax.all_gather(key_value, 'ep', axis=0, tiled=True)]
    all_to_all x1 -> x0, starting transfers between devices: 16.7 us -> none  [on_device(): lax.all_to_all(own_columns[sources], 'ep', split_axis=0, concat_axis=0, t...]
  transfers between devices with their start and end apart: 6 -> 5, of which waited for: 4 -> 4; matrix products, arithmetic and copies ran while one was open for 43% -> 11% of each run, Pallas kernels for 0% -> 11%
where the time goes in v1:
time: 328 us; the launch traced here: 327 us
  waiting for transfers between devices  150 us (46%)
  blocking collectives  57.5 us (18%)
  local copies, waits for them, and re-layouts  36.9 us (11%)
  Pallas kernels  35.5 us (11%)
  starting transfers between devices  15.2 us (5%)
  between operations  14.1 us (4%)
  matrix products  11 us (3%)
  other arithmetic  7.26 us (2%)
    all_gather x1, waiting for transfers between devices, on_device(): incoming = lax.all_gather(received, TP, axis=3, tiled=True)  67.1 us
    all_gather x1, waiting for transfers between devices, on_device(): incoming = lax.all_gather(key_value, 'ep', axis=0, tiled=True)  58 us
    all_to_all x1, blocking collectives, on_device(): lax.all_to_all(own_columns[sources], 'ep', split_axis=0, concat_axis=0, t...  44.4 us
    pallas_call x1, Pallas kernels, flash(): pl.pallas_call(functools.partial(flash_kernel, width, block), out_shape=j...  33.5 us
    all_to_all x1, waiting for transfers between devices, on_device(): lax.all_to_all(expert_out, 'ep', split_axis=0, concat_axis=0, tiled=True)  16.2 us
    unnamed x38, local copies, waits for them, and re-layouts  15.4 us
    all_gather x1, blocking collectives, gather_axes(): x = lax.all_gather(x, axis, axis=dim, tiled=True)  13.1 us
    all_to_all x1, starting transfers between devices, on_device(): lax.all_to_all(expert_out, 'ep', split_axis=0, concat_axis=0, tiled=True)  10.4 us
  transfers between devices with their start and end apart: 5, of which 4 were waited for; matrix products, arithmetic and copies ran while one was open for 11% of the time, Pallas kernels for 11%

profile of v1, /device:TPU:1, one launch (start us, length us, event | category | flops | bytes accessed | tf_op | source)
XLA Modules:
  0.0 327.1 jit_solution(11237494958649177584)
XLA Ops:
  7.2 0.0 all-gather.9.cloned.1.call-start
  7.3 1.0 copy.34
  8.2 0.1 eq.31
  8.4 0.1 eq.27
  8.5 0.7 broadcast_multiply_fusion.2
  9.2 2.1 fusion
  11.3 1.2 reduce-window.6
  12.5 0.2 slice_reduce_fusion
  12.7 0.1 copy.33
  12.9 0.1 mul.103
  13.0 0.1 fusion.11
  13.2 2.4 scatter_custom_fusion
  15.7 0.7 fusion.2
  16.5 2.7 gather_fusion
  19.2 44.4 %all_to_all.23 = bf16[32,24,256]{2,1,0:T(8,128)(2,1)} all-to-all(bf16[32,24,256]{2,1,0:T(8,128)(2,1)S(1)} %bitcast.73), channel_id=1, replica_groups=mesh['ep'=32,'tp_0'=4,'tp_1'=4] {'ep'}, dimensions={0} | all-to-all | bytes 786432 | tf_op jit(solution)/shard_map/all_to_all | solution.py:219
  63.6 0.0 all-gather.5.cloned.1.call-start
  63.7 0.8 copy.29.k_ref
  64.4 0.8 copy.30.v_ref
  65.2 0.7 copy.31.gain_ref
  65.9 0.1 broadcast_multiply_fusion.1
  66.0 0.9 fusion.13
  66.9 2.0 shard_map.140
  68.9 0.1 copy.32.gain_ref
  69.0 67.1 %all-gather.9.cloned.1.call-done = bf16[32,24,4096]{2,1,0:T(8,128)(2,1)} async-done(((bf16[32,24,256]{2,1,0:T(8,128)(2,1)}), bf16[32,24,4096]{2,1,0:T(8,128)(2,1)}) %all-gather.9.cloned.1.call-update) | async-done | bytes 6291472 | tf_op jit(solution)/shard_map/all_gather | solution.py:221
  136.0 4.7 %convolution_bitcast_fusion.1 = f32[32,1,24,64]{3,2,0,1:T(8,128)S(1)} fusion(bf16[32,24,4096]{2,1,0:T(8,128)(2,1)} %all-gather.9.cloned.1.call-done, bf16[1,4096,64]{1,2,0:T(8,128)(2,1)S(1)} %copy-done.13), kind=kOutput, calls=%fused_computation.12 | convolution fusion | flops 402653184 | bytes 7012352 | tf_op jit(solution)/shard_map/sjcd,jdf->sjcf/dot_general | solution.py:222
  140.8 1.9 fusion.5
  142.7 2.3 broadcast_bitcast_fusion
  145.0 5.0 %reshape.178 = bf16[16,2,24576]{2,1,0:T(2,128)(2,1)} reshape(bf16[16,1,32,24,64]{4,3,2,1,0:T(8,128)(2,1)} %broadcast_bitcast_fusion) | data formatting | bytes 3145728
  150.0 4.7 %all-to-all-start.1 = ((bf16[16,2,24576]{2,1,0:T(2,128)(2,1)}), bf16[16,2,24576]{2,1,0:T(2,128)(2,1)S(1)}, u32[]{:S(2)}, u32[]{:S(2)}) async-start(bf16[16,2,24576]{2,1,0:T(2,128)(2,1)} %reshape.178), calls=%async_computation.1 | async-start | bytes 3145728 | tf_op jit(solution)/shard_map/all_to_all | solution.py:27
  154.7 0.0 all-gather.7.cloned.1.call-start
  154.8 58.0 %all-gather.5.cloned.1.call-done.kv_ref = bf16[16384,128]{1,0:T(8,128)(2,1)} async-done(((bf16[512,128]{1,0:T(8,128)(2,1)}), bf16[16384,128]{1,0:T(8,128)(2,1)}) %all-gather.5.cloned.1.call-update) | async-done | bytes 4194320 | tf_op jit(solution)/shard_map/all_gather | solution.py:195
  212.8 2.2 copy-done.3
  215.0 33.5 %shard_map.141 = bf16[512,128]{1,0:T(8,128)(2,1)S(1)} custom-call(bf16[512,128]{1,0:T(8,128)(2,1)S(1)} %copy-done.4, bf16[16384,128]{1,0:T(8,128)(2,1)S(1)} %copy-done.3, f32[32,512]{1,0:T(8,128)S(1)} %copy-done.2, f32[32,512]{1,0:T(8,128)S(1)} %copy-done.1, f32[64,1]{1,0:T(8,128)S(1)} %copy.32.gain_ref), custom_call_target="tpu_custom_call" | custom-call | flops 20000000000 | bytes 5000000 | tf_op jit(solution)/shard_map/pallas_call | solution.py:141
  248.5 13.1 %all_gather.13 = bf16[512,512]{1,0:T(8,128)(2,1)} all-gather(bf16[512,128]{1,0:T(8,128)(2,1)S(1)} %shard_map.141), channel_id=1, replica_groups=mesh['ep'=32,'tp_0'=4,'tp_1'=4] {'tp_1'}, dimensions={1}, use_global_device_ids=true | all-gather | bytes 655360 | tf_op jit(solution)/shard_map/all_gather | solution.py:21
  261.6 0.0 all-gather.7.cloned.1.call-update
  261.6 3.4 %reshape.179 = bf16[16,1,32,24,64]{4,3,2,1,0:T(8,128)(2,1)} reshape(bf16[16,2,24576]{2,1,0:T(2,128)(2,1)S(1)} %all-to-all-done.1) | data formatting | bytes 3145728
  265.0 2.6 bitcast_bitcast_fusion.1
  267.6 5.3 %copy.37 = bf16[32,1,24,16,64]{4,3,2,0,1:T(8,128)(2,1)} copy(bf16[32,1,24,16,64]{4,2,0,1,3:T(8,128)(2,1)S(1)} %bitcast_bitcast_fusion.1) | data formatting | bytes 3145728 | tf_op jit(solution)/shard_map/transpose | solution.py:31
  272.9 4.6 %reshape.142 = bf16[32,24,1024]{2,1,0:T(8,128)(2,1)S(1)} reshape(bf16[32,1,24,16,64]{4,3,2,0,1:T(8,128)(2,1)} %copy.37) | data formatting | bytes 3145728 | tf_op jit(solution)/shard_map/reshape.18
  277.5 1.3 convolution_convert_fusion
  278.8 10.4 %all-to-all-start.2 = ((bf16[32,24,256]{2,1,0:T(8,128)(2,1)}), bf16[32,24,256]{2,1,0:T(8,128)(2,1)S(1)}, u32[]{:S(2)}, u32[]{:S(2)}) async-start(bf16[32,24,256]{2,1,0:T(8,128)(2,1)} %convolution_convert_fusion), calls=%async_computation.2 | async-start | bytes 786432 | tf_op jit(solution)/shard_map/all_to_all | solution.py:238
  289.2 0.1 copy.38
  289.4 8.4 %all-gather.7.cloned.1.call-done = bf16[512,2048]{1,0:T(8,128)(2,1)} async-done(((bf16[512,512]{1,0:T(8,128)(2,1)}), bf16[512,2048]{1,0:T(8,128)(2,1)}) %all-gather.7.cloned.1.call-update) | async-done | bytes 2097168 | tf_op jit(solution)/shard_map/all_gather | solution.py:21
  297.8 3.0 convolution_convert_fusion.1
  300.8 16.2 %all-to-all-done.2 = bf16[32,24,256]{2,1,0:T(8,128)(2,1)S(1)} async-done(((bf16[32,24,256]{2,1,0:T(8,128)(2,1)}), bf16[32,24,256]{2,1,0:T(8,128)(2,1)S(1)}, u32[]{:S(2)}, u32[]{:S(2)}) %all-to-all-start.2) | async-done | bytes 393248 | tf_op jit(solution)/shard_map/all_to_all | solution.py:238
  316.9 1.9 gather_fusion.1
  318.9 0.3 reshape.144
  319.2 1.4 multiply_reduce_fusion
  (48 shorter events, 0.3 us)
Async XLA Ops:
  7.2 290.6 %copy-start = (bf16[2048,256]{1,0:T(8,128)(2,1)S(1)}, bf16[2048,256]{1,0:T(8,128)(2,1)}, u32[]{:S(2)}) copy-start(bf16[2048,256]{1,0:T(8,128)(2,1)} %param.18) | copy-start | bytes 3145732
  7.2 8.5 %copy-start.5 = (bf16[256,4096]{1,0:T(8,128)(2,1)S(1)}, bf16[256,4096]{1,0:T(8,128)(2,1)}, u32[]{:S(2)}) copy-start(bf16[256,4096]{1,0:T(8,128)(2,1)} %param.19) | copy-start | bytes 6291460
  7.2 8.5 %copy-start.8 = (f32[4096]{0:T(1024)S(1)}, f32[4096]{0:T(1024)}, u32[]{:S(2)}) copy-start(f32[4096]{0:T(1024)} %param.20) | copy-start | bytes 49156
  7.2 128.8 %all-gather.9.cloned.1.call-start = ((), (), s32[]{:S(2)}) async-start(), calls=%async_computation.5 | async-start | bytes 6684672 | tf_op jit(solution)/shard_map/all_gather | solution.py:221
  16.4 47.2 %copy-start.6 = (bf16[512,64]{0,1:T(8,128)(2,1)S(1)}, bf16[512,64]{0,1:T(8,128)(2,1)}, u32[]{:S(2)}) copy-start(bf16[512,64]{0,1:T(8,128)(2,1)} %param.14) | copy-start | bytes 196612
  16.4 48.0 %copy-start.7 = (bf16[512,64]{0,1:T(8,128)(2,1)S(1)}, bf16[512,64]{0,1:T(8,128)(2,1)}, u32[]{:S(2)}) copy-start(bf16[512,64]{0,1:T(8,128)(2,1)} %param.15) | copy-start | bytes 196612
  16.4 48.7 %copy-start.10 = (f32[64]{0:T(128)S(1)}, f32[64]{0:T(128)}, u32[]{:S(2)}) copy-start(f32[64]{0:T(128)} %param.17) | copy-start | bytes 772
  16.5 52.4 %copy-start.11 = (f32[64]{0:T(128)S(1)}, f32[64]{0:T(128)}, u32[]{:S(2)}) copy-start(f32[64]{0:T(128)} %param.16) | copy-start | bytes 772
  16.5 119.5 %copy-start.13 = (bf16[1,4096,64]{1,2,0:T(8,128)(2,1)S(1)}, bf16[1,4096,64]{1,2,0:T(8,128)(2,1)}, u32[]{:S(2)}) copy-start(bf16[1,4096,64]{1,2,0:T(8,128)(2,1)} %param.23) | copy-start | bytes 1572868
  63.6 149.2 %all-gather.5.cloned.1.call-start = ((), (), s32[]{:S(2)}) async-start(), calls=%async_computation.3 | async-start | bytes 4325376 | tf_op jit(solution)/shard_map/all_gather | solution.py:195
  69.0 71.8 %copy-start.14 = (bf16[1,4096,64]{1,2,0:T(8,128)(2,1)S(1)}, bf16[1,4096,64]{1,2,0:T(8,128)(2,1)}, u32[]{:S(2)}) copy-start(bf16[1,4096,64]{1,2,0:T(8,128)(2,1)} %param.24) | copy-start | bytes 1572868
  136.0 4.7 %copy-start.12 = (bf16[32,24,4096]{2,1,0:T(8,128)(2,1)S(1)}, bf16[32,24,4096]{2,1,0:T(8,128)(2,1)}, u32[]{:S(2)}) copy-start(bf16[32,24,4096]{2,1,0:T(8,128)(2,1)} %all-gather.9.cloned.1.call-done) | copy-start | bytes 18874372
  145.0 67.7 %copy-start.1 = (f32[32,512]{1,0:T(8,128)S(1)}, f32[32,512]{1,0:T(8,128)}, u32[]{:S(2)}) copy-start(f32[32,512]{1,0:T(8,128)} %get-tuple-element.2.sin_ref) | copy-start | bytes 196612
  145.0 67.7 %copy-start.2 = (f32[32,512]{1,0:T(8,128)S(1)}, f32[32,512]{1,0:T(8,128)}, u32[]{:S(2)}) copy-start(f32[32,512]{1,0:T(8,128)} %get-tuple-element.3.cos_ref) | copy-start | bytes 196612
  145.0 67.7 %copy-start.4 = (bf16[512,128]{1,0:T(8,128)(2,1)S(1)}, bf16[512,128]{1,0:T(8,128)(2,1)}, u32[]{:S(2)}) copy-start(bf16[512,128]{1,0:T(8,128)(2,1)} %q_ref.1) | copy-start | bytes 393220
  150.0 111.6 %all-to-all-start.1 = ((bf16[16,2,24576]{2,1,0:T(2,128)(2,1)}), bf16[16,2,24576]{2,1,0:T(2,128)(2,1)S(1)}, u32[]{:S(2)}, u32[]{:S(2)}) async-start(bf16[16,2,24576]{2,1,0:T(2,128)(2,1)} %reshape.178), calls=%async_computation.1 | async-start | bytes 3145728 | tf_op jit(solution)/shard_map/all_to_all | solution.py:27
  154.7 143.0 %all-gather.7.cloned.1.call-start = ((), (), s32[]{:S(2)}) async-start(), calls=%async_computation.4 | async-start | bytes 2621440 | tf_op jit(solution)/shard_map/all_gather | solution.py:21
  212.8 2.2 copy-start.3
  272.9 4.6 %copy-start.15 = (bf16[1,1024,256]{2,1,0:T(8,128)(2,1)S(1)}, bf16[1,1024,256]{2,1,0:T(8,128)(2,1)}, u32[]{:S(2)}) copy-start(bf16[1,1024,256]{2,1,0:T(8,128)(2,1)} %param.25) | copy-start | bytes 1572868
  272.9 16.3 %copy-start.9 = (f32[256,2]{0,1:T(2,128)S(1)}, f32[256,2]{0,1:T(2,128)}, u32[]{:S(2)}) copy-start(f32[256,2]{0,1:T(2,128)} %param.22) | copy-start | bytes 6148
  278.8 38.1 %all-to-all-start.2 = ((bf16[32,24,256]{2,1,0:T(8,128)(2,1)}), bf16[32,24,256]{2,1,0:T(8,128)(2,1)S(1)}, u32[]{:S(2)}, u32[]{:S(2)}) async-start(bf16[32,24,256]{2,1,0:T(8,128)(2,1)} %convolution_convert_fusion), calls=%async_computation.2 | async-start | bytes 786432 | tf_op jit(solution)/shard_map/all_to_all | solution.py:238
Sparse Core Ops, SparseCore 0:
  63.7 72.2 all-gather.8
  138.1 74.5 all-gather.4
  261.7 35.9 all-gather.6

commit v2 on v1

v2 whole, which is shorter than its diff:
```python
import functools

import jax
import jax.numpy as jnp
from jax import lax
from jax.experimental import pallas as pl
from jax.experimental.pallas import tpu as pltpu
from jax.sharding import Mesh
from jax.sharding import PartitionSpec as P

GRID_W = 64
TOP_K = 2
CORES = 2
GROUPS = 4
AXES = ("z", "c", "y", "x")
epsilon = 1e-06
base_theta = 10000.0
log2e = 1.4426950408889634
MESH = pl.DeviceIdType.MESH


def rope_tables(positions, head_width):
    quarter = head_width // 4
    inverse = base_theta ** (-jnp.arange(quarter, dtype=jnp.float32) / quarter)
    grid_row = (positions // GRID_W).astype(jnp.float32)
    grid_col = (positions % GRID_W).astype(jnp.float32)
    angles = jnp.concatenate(
        [inverse[:, None] * grid_row[None, :], inverse[:, None] * grid_col[None, :]], axis=0
    )
    return (jnp.cos(angles), jnp.sin(angles))


def rotated(x, cosine, sine, gain):
    scale = lax.rsqrt(jnp.mean(x * x, axis=0, keepdims=True) + epsilon)
    x = x * scale * gain
    half = x.shape[0] // 2
    first, second = x[:half], x[half:]
    return jnp.concatenate(
        [first * cosine - second * sine, first * sine + second * cosine], axis=0
    )


def ring_offsets(size):
    offsets = [0]
    for step in range(1, size // 2 + 1):
        offsets.append(step)
        if step < size - step:
            offsets.append(-step)
    return offsets


def step_kernel(
    sizes,
    cap,
    q_ref,
    k_ref,
    v_ref,
    cos_ref,
    sin_ref,
    qg_ref,
    kg_ref,
    x_ref,
    xg_ref,
    routes_ref,
    share_ref,
    mixer_hbm,
    gate_hbm,
    up_hbm,
    down_hbm,
    attn_ref,
    moe_ref,
    kv_ref,
    qt_ref,
    s0_ref,
    s1_ref,
    x0_ref,
    x1_ref,
    m_ref,
    o_ref,
    named_ref,
    count_ref,
    weight_ref,
    pick_ref,
    combine_ref,
    chi_ref,
    clo_ref,
    disp_ref,
    rows_ref,
    gu_ref,
    acc_ref,
    hid_ref,
    eo_ref,
    back_ref,
    att_ref,
    mixer_ref,
    gate_ref,
    up_ref,
    down_ref,
    load_sem,
    kv_send,
    kv_recv,
    d_send,
    d_recv,
    r_send,
    r_recv,
    g1_send,
    g1_recv,
    g2_send,
    g2_recv,
    a1_send,
    a1_recv,
    a2_send,
    a2_recv,
    h1_send,
    h1_recv,
    h2_send,
    h2_recv,
):
    Z, Y, X = sizes
    T = Y * X
    experts = Z * CORES
    z, c = lax.axis_index("z"), lax.axis_index("c")
    y, x = lax.axis_index("y"), lax.axis_index("x")
    ep = z * CORES + c
    tp = y * X + x
    offsets = ring_offsets(Z)
    places = [(rel, dc) for rel in offsets for dc in range(CORES)]
    block = 2 * cap
    f32, bf16 = jnp.float32, jnp.bfloat16

    def line(rel, dc):
        return {"z": lax.rem(z + (rel + Z), Z), "c": lax.rem(c + dc, CORES)}

    def x_peer(dx):
        return {"x": lax.rem(x + (dx + X), X)}

    def y_peer(dy):
        return {"y": lax.rem(y + (dy + Y), Y)}

    barrier = pltpu.get_barrier_semaphore()
    greeted = 0
    for rel, dc in places[1:]:
        pl.semaphore_signal(barrier, inc=1, device_id=line(rel, dc), device_id_type=MESH)
        greeted += 1
    for dx in range(1, X):
        pl.semaphore_signal(barrier, inc=1, device_id=x_peer(dx), device_id_type=MESH)
        greeted += 1
    for dy in range(1, Y):
        pl.semaphore_signal(barrier, inc=1, device_id=y_peer(dy), device_id_type=MESH)
        greeted += 1

    loads = [
        pltpu.make_async_copy(gate_hbm, gate_ref, load_sem.at[0]),
        pltpu.make_async_copy(up_hbm, up_ref, load_sem.at[1]),
        pltpu.make_async_copy(down_hbm, down_ref, load_sem.at[2]),
        pltpu.make_async_copy(mixer_hbm, mixer_ref, load_sem.at[3]),
    ]
    for load in loads:
        load.start()

    def remote(src, dst, send, recv, device):
        return pltpu.make_async_remote_copy(
            src_ref=src, dst_ref=dst, send_sem=send, recv_sem=recv, device_id=device, device_id_type=MESH
        )

    rows, features = x_ref.shape
    share = features // T
    half = share // 2
    expert_at = lax.broadcasted_iota(jnp.int32, (experts, rows), 0)
    first = routes_ref[0:1, :] == expert_at
    second = routes_ref[1:2, :] == expert_at
    total_share = share_ref[0:1, :] + share_ref[1:2, :]
    named = jnp.where(first | second, 1.0, 0.0)
    earlier = jnp.where(
        lax.broadcasted_iota(jnp.int32, (rows, rows), 0)
        < lax.broadcasted_iota(jnp.int32, (rows, rows), 1),
        1.0,
        0.0,
    ).astype(bf16)
    count = jnp.dot(named.astype(bf16), earlier, preferred_element_type=f32)
    named_ref[...] = named
    count_ref[...] = jnp.where(named > 0.0, count, -1.0)
    weight_ref[...] = jnp.where(first, share_ref[0:1, :] / total_share, 0.0) + jnp.where(
        second, share_ref[1:2, :] / total_share, 0.0
    )
    slot_at = lax.broadcasted_iota(jnp.int32, (block, rows), 0)
    slot_at = jnp.where(slot_at < cap, slot_at, slot_at - cap).astype(f32)

    @pl.loop(0, experts)
    def _(expert):
        here = count_ref[pl.ds(expert, 1), :] == slot_at
        at = pl.ds(pl.multiple_of(expert * block, block), block)
        pick_ref[at, :] = jnp.where(here, 1.0, 0.0).astype(bf16)
        combine_ref[at, :] = jnp.where(here, weight_ref[pl.ds(expert, 1), :], 0.0)

    chunk = 512
    squares = jnp.zeros((rows, 128), f32)
    for start in range(0, features, chunk):
        part = x_ref[:, start : start + chunk].astype(f32)
        part = part * part
        for lane in range(0, chunk, 128):
            squares = squares + part[:, lane : lane + 128]
    mean = jnp.sum(squares, axis=1, keepdims=True) * (1.0 / features)
    own = pl.ds(pl.multiple_of(tp * share, share), share)
    normed = (x_ref[:, own].astype(f32) * lax.rsqrt(mean + epsilon) * xg_ref[:, own]).astype(bf16)
    picked = jnp.dot(pick_ref[...], normed, preferred_element_type=f32)
    picked = picked.reshape(experts, block, share)
    picked = jnp.concatenate([picked[:, :cap, :half], picked[:, cap:, half:]], axis=1)
    disp_ref[...] = picked.reshape(experts * block, half).astype(bf16)

    width = k_ref.shape[1]
    k_t = rotated(k_ref[...].astype(f32).T, cos_ref[...], sin_ref[...], kg_ref[...])
    kv_ref[0] = jnp.concatenate([k_t.T, v_ref[...].astype(f32)], axis=1).astype(bf16)

    pl.semaphore_wait(barrier, greeted)

    def expert_rows(rel, dc):
        target = line(rel, dc)
        return pl.ds(pl.multiple_of((target["z"] * CORES + target["c"]) * block, block), block)

    def dispatch(p):
        rel, dc = places[p]
        return remote(
            disp_ref.at[expert_rows(-rel, dc)],
            rows_ref.at[y, x, pl.ds(p * block, block)],
            d_send.at[p],
            d_recv.at[p],
            line(-rel, dc),
        )

    kept = pltpu.make_async_copy(
        disp_ref.at[expert_rows(0, 0)], rows_ref.at[y, x, pl.ds(0, block)], d_recv.at[0]
    )
    kept.start()
    for p in range(1, len(places)):
        dispatch(p).start()

    def base(step):
        return 2 + 4 * (step - 1)

    last = Z // 2
    tail = base(last)

    def rightward(step):
        src = lax.select(step == 1, 0, base(step - 1)) if not isinstance(step, int) else (
            0 if step == 1 else base(step - 1)
        )
        return remote(kv_ref.at[src], kv_ref.at[base(step)], kv_send.at[base(step)], kv_recv.at[base(step)], line(1, 0))

    def leftward(step):
        src = lax.select(step == 1, 0, base(step - 1) + 1) if not isinstance(step, int) else (
            0 if step == 1 else base(step - 1) + 1
        )
        to = base(step) + 1
        return remote(kv_ref.at[src], kv_ref.at[to], kv_send.at[to], kv_recv.at[to], line(-1, 0))

    def across(src, to):
        return remote(kv_ref.at[src], kv_ref.at[to], kv_send.at[to], kv_recv.at[to], line(0, 1))

    rightward(1).start()
    leftward(1).start()
    across(0, 1).start()

    tokens = q_ref.shape[0]
    heads = q_ref.shape[1] // width
    lanes = heads * tokens
    q_t = q_ref[...].astype(f32).T
    for head in range(heads):
        turned = rotated(
            q_t[head * width : (head + 1) * width], cos_ref[...], sin_ref[...], qg_ref[...]
        )
        turned = turned.astype(bf16).astype(f32) * (width ** (-0.5))
        qt_ref[:width, head * tokens : (head + 1) * tokens] = turned.astype(bf16)
    qt_ref[width:, :] = jnp.zeros((width, lanes), bf16)
    m_ref[...] = jnp.full(m_ref.shape, -1e30, f32)
    o_ref[...] = jnp.zeros(o_ref.shape, f32)
    s_ref, mx_ref = (s0_ref, s1_ref), (x0_ref, x1_ref)

    def scores(slot, buffer):
        s = jnp.dot(kv_ref[slot], qt_ref[...], preferred_element_type=f32)
        s_ref[buffer][...] = s
        mx_ref[buffer][...] = jnp.max(s.reshape(tokens // 8, 8, lanes), axis=0)

    def absorb(slot, buffer):
        old = m_ref[...]
        new = jnp.maximum(old, jnp.max(mx_ref[buffer][...], axis=0, keepdims=True) * log2e)
        m_ref[...] = new
        factor = jnp.exp2(old - new)
        p = jnp.exp2(s_ref[buffer][...] * log2e - new[:1]).astype(bf16)
        v_t = kv_ref[slot].T[width:]
        lhs = jnp.concatenate([jnp.ones((16, tokens), bf16), v_t], axis=0)
        part = jnp.dot(lhs, p, preferred_element_type=f32)
        o_ref[...] = o_ref[...] * factor[:1] + part

    def along_x(ref, piece, send, recv, n):
        return [
            (
                remote(ref.at[y, x, piece], ref.at[y, x, piece], send.at[n, dx - 1], recv.at[n, dx - 1], x_peer(dx)),
                remote(
                    ref.at[y, x_peer(-dx)["x"], piece],
                    ref.at[y, x_peer(-dx)["x"], piece],
                    send.at[n, dx - 1],
                    recv.at[n, dx - 1],
                    x_peer(dx),
                ),
            )
            for dx in range(1, X)
        ]

    def along_y(ref, piece, send, recv, n):
        return [
            (
                remote(ref.at[y, x, piece], ref.at[y, x, piece], send.at[n, dy - 1], recv.at[n, dy - 1], y_peer(dy)),
                remote(
                    ref.at[y_peer(-dy)["y"], x, piece],
                    ref.at[y_peer(-dy)["y"], x, piece],
                    send.at[n, dy - 1],
                    recv.at[n, dy - 1],
                    y_peer(dy),
                ),
            )
            for dy in range(1, Y)
        ]

    def then_y(ref, piece, send, recv, n):
        every = pl.ds(0, X)
        return [
            (
                remote(ref.at[y, every, piece], ref.at[y, every, piece], send.at[n, dy - 1], recv.at[n, dy - 1], y_peer(dy)),
                remote(
                    ref.at[y_peer(-dy)["y"], every, piece],
                    ref.at[y_peer(-dy)["y"], every, piece],
                    send.at[n, dy - 1],
                    recv.at[n, dy - 1],
                    y_peer(dy),
                ),
            )
            for dy in range(1, Y)
        ]

    def then_x(ref, piece, send, recv, n):
        every = pl.ds(0, Y)
        return [
            (
                remote(ref.at[every, x, piece], ref.at[every, x, piece], send.at[n, dx - 1], recv.at[n, dx - 1], x_peer(dx)),
                remote(
                    ref.at[every, x_peer(-dx)["x"], piece],
                    ref.at[every, x_peer(-dx)["x"], piece],
                    send.at[n, dx - 1],
                    recv.at[n, dx - 1],
                    x_peer(dx),
                ),
            )
            for dx in range(1, X)
        ]

    def hops(ref, piece, n, send1, recv1, send2, recv2):
        if n % 2 == 0:
            return along_x(ref, piece, send1, recv1, n), then_y(ref, piece, send2, recv2, n)
        return along_y(ref, piece, send1, recv1, n), then_x(ref, piece, send2, recv2, n)

    def start(copies):
        for out, _ in copies:
            out.start()

    def arrive(copies):
        for _, into in copies:
            into.wait_recv()

    def sent(copies):
        for out, _ in copies:
            out.wait_send()

    per_group = len(places) // GROUPS
    span = per_group * block

    def rows_hops(group):
        return hops(rows_ref, pl.ds(group * span, span), group, g1_send, g1_recv, g2_send, g2_recv)

    def group_arrived(group):
        for p in range(group * per_group, (group + 1) * per_group):
            if p == 0:
                kept.wait()
            else:
                dispatch(p).wait_recv()
        start(rows_hops(group)[0])

    def group_forwarded(group):
        first_hop, second_hop = rows_hops(group)
        arrive(first_hop)
        start(second_hop)

    scores(0, 0)
    across(0, 1).wait_recv()
    scores(1, 1)
    absorb(0, 0)

    for load in loads:
        load.wait()
    for t in range(T):
        top, low = t * share, t * share + half
        gu_ref[t * half : (t + 1) * half, :] = jnp.concatenate(
            [
                gate_ref[top : top + half, :],
                up_ref[top : top + half, :],
                gate_ref[low : low + half, :],
                up_ref[low : low + half, :],
            ],
            axis=1,
        )
    for e in range(0, experts * block, 256):
        turned = combine_ref[e : e + 256, :].T
        high = turned.astype(bf16)
        chi_ref[:, e : e + 256] = high
        clo_ref[:, e : e + 256] = (turned - high.astype(f32)).astype(bf16)

    @pl.loop(1, last)
    def _(step):
        at = base(step)
        rightward(step).wait_recv()
        rightward(step + 1).start()
        across(at, at + 2).start()
        leftward(step).wait_recv()

        @pl.when(step < last - 1)
        def _():
            leftward(step + 1).start()

        across(at + 1, at + 3).start()
        for group in range(GROUPS):

            @pl.when(step == min(group + 1, last - 1))
            def _(group=group):
                group_arrived(group)

            @pl.when(step == min(group + 2, last - 1))
            def _(group=group):
                group_forwarded(group)

        @pl.loop(0, 2)
        def _(pair):
            even = at + 2 * pair

            @pl.when(pair == 1)
            def _():
                across(at, at + 2).wait_recv()
                across(at + 1, at + 3).wait_recv()

            scores(even, 0)
            absorb(even - 1, 1)
            scores(even + 1, 1)
            absorb(even, 0)

    rightward(last).wait_recv()
    across(tail, tail + 1).start()
    scores(tail, 0)
    absorb(tail - 1, 1)
    across(tail, tail + 1).wait_recv()
    scores(tail + 1, 1)
    absorb(tail, 0)
    absorb(tail + 1, 1)

    attended = o_ref[16:, :] / o_ref[:1, :]
    for head in range(heads):
        piece = attended[:, head * tokens : (head + 1) * tokens].T
        att_ref[y, x, :, head * width : (head + 1) * width] = piece.astype(bf16)
    att_half = tokens // 2
    att_hops = [
        hops(att_ref, pl.ds(n * att_half, att_half), n, a1_send, a1_recv, a2_send, a2_recv)
        for n in range(2)
    ]
    for n in range(2):
        start(att_hops[n][0])

    hidden_width = gate_ref.shape[1]
    pack = per_group * cap // 2
    for group in range(GROUPS):
        arrive(rows_hops(group)[1])
        at = pl.ds(group * span, span)
        total = None
        for t in range(0, T, min(T, 4)):
            many = range(t, min(t + 4, T))
            lhs = jnp.concatenate([rows_ref[u // X, u % X, at, :] for u in many], axis=1)
            term = jnp.dot(
                lhs, gu_ref[t * half : (t + len(many)) * half, :], preferred_element_type=f32
            )
            total = term if total is None else total + term
        both = total.reshape(per_group, block, 4 * hidden_width)
        both = both[:, :cap, : 2 * hidden_width] + both[:, cap:, 2 * hidden_width :]
        both = both.reshape(per_group * cap, 2 * hidden_width)
        gate = both[:, :hidden_width]
        up = both[:, hidden_width:]
        hidden = gate / (1.0 + jnp.exp(-gate)) * up
        hidden = jnp.concatenate([hidden[:pack], hidden[pack:]], axis=1)
        hid_ref[y, x, group * pack : (group + 1) * pack, :] = hidden.astype(bf16)
    hid_half = GROUPS * pack // 2
    hid_hops = [
        hops(hid_ref, pl.ds(n * hid_half, hid_half), n, h1_send, h1_recv, h2_send, h2_recv)
        for n in range(2)
    ]
    for n in range(2):
        start(hid_hops[n][0])
    for n in range(2):
        arrive(hid_hops[n][0])
        start(hid_hops[n][1])
    for n in range(2):
        arrive(att_hops[n][0])
        start(att_hops[n][1])

    def giveback(p):
        rel, dc = places[p]
        mine = pl.ds(pl.multiple_of(ep * block, block), block)
        return remote(
            eo_ref.at[pl.ds(p * block, block)], back_ref.at[mine], r_send.at[p], r_recv.at[p], line(rel, dc)
        )

    def returned(p):
        rel, dc = places[p]
        at = expert_rows(-rel, dc)
        return remote(back_ref.at[at], back_ref.at[at], r_send.at[p], r_recv.at[p], line(rel, dc))

    mine = pl.ds(pl.multiple_of(ep * block, block), block)
    own_back = pltpu.make_async_copy(eo_ref.at[pl.ds(0, block)], back_ref.at[mine], r_recv.at[0])
    for n in range(2):
        arrive(hid_hops[n][1])
        for group in range(n * GROUPS // 2, (n + 1) * GROUPS // 2):
            lo = jnp.concatenate(
                [hid_ref[u // X, u % X, group * pack : (group + 1) * pack, :hidden_width] for u in range(T)],
                axis=1,
            )
            hi = jnp.concatenate(
                [hid_ref[u // X, u % X, group * pack : (group + 1) * pack, hidden_width:] for u in range(T)],
                axis=1,
            )
            out = jnp.dot(
                jnp.concatenate([lo, hi], axis=0), down_ref[...], preferred_element_type=f32
            )
            out = out.reshape(per_group, cap, share)
            out = jnp.concatenate([out[:, :, :half], out[:, :, half:]], axis=1)
            eo_ref[group * span : (group + 1) * span, :] = out.reshape(span, half).astype(bf16)
            for p in range(group * per_group, (group + 1) * per_group):
                if p == 0:
                    own_back.start()
                else:
                    giveback(p).start()

    for n in range(2):
        arrive(att_hops[n][1])
        at = pl.ds(n * att_half, att_half)
        lhs = jnp.concatenate([att_ref[u // X, u % X, at, :] for u in range(T)], axis=1)
        attn_ref[n * att_half : (n + 1) * att_half, :] = jnp.dot(
            lhs, mixer_ref[...], preferred_element_type=f32
        ).astype(bf16)

    own_back.wait()
    for p in range(1, len(places)):
        returned(p).wait_recv()
    back = back_ref[...].astype(f32).reshape(experts, block, half)
    blank = jnp.zeros((experts, cap, half), f32)
    wide = jnp.concatenate(
        [
            jnp.concatenate([back[:, :cap], blank], axis=1),
            jnp.concatenate([blank, back[:, cap:]], axis=1),
        ],
        axis=2,
    )
    wide = wide.reshape(experts * block, share).astype(bf16)
    moe = jnp.dot(chi_ref[...], wide, preferred_element_type=f32)
    moe = moe + jnp.dot(clo_ref[...], wide, preferred_element_type=f32)
    moe_ref[...] = moe.astype(bf16)

    across(0, 1).wait_send()
    for step in range(1, last + 1):
        rightward(step).wait_send()
        if step < last:
            leftward(step).wait_send()
            across(base(step), base(step) + 2).wait_send()
            across(base(step) + 1, base(step) + 3).wait_send()
    across(tail, tail + 1).wait_send()
    for p in range(1, len(places)):
        dispatch(p).wait_send()
        giveback(p).wait_send()
    for group in range(GROUPS):
        for copies in rows_hops(group):
            sent(copies)
    for n in range(2):
        for copies in att_hops[n] + hid_hops[n]:
            sent(copies)


def on_device(
    sizes,
    query_input,
    key_input,
    value_input,
    query_gain,
    key_gain,
    mixer_out,
    moe_input,
    moe_gain,
    routes,
    route_weight,
    expert_gate,
    expert_up,
    expert_down,
):
    Z, Y, X = sizes
    T = Y * X
    experts = Z * CORES
    tokens, columns = query_input.shape
    width = query_gain.shape[0]
    lanes = tokens * (columns // width)
    ep = lax.axis_index("z") * CORES + lax.axis_index("c")
    positions = ep * tokens + jnp.arange(tokens, dtype=jnp.int32)
    cosine, sine = rope_tables(positions, width)
    rows, features = moe_input.shape
    share = features // T
    half = share // 2
    cap = 3 * rows * TOP_K // (2 * experts)
    block = 2 * cap
    hidden = expert_gate.shape[2]
    gate, up, down = expert_gate[0], expert_up[0], expert_down[0]
    vmem = pl.BlockSpec(memory_space=pltpu.VMEM)
    hbm = pl.BlockSpec(memory_space=pl.ANY)
    bf16, f32 = jnp.bfloat16, jnp.float32
    dma = pltpu.SemaphoreType.DMA
    last = Z // 2
    slots = experts
    total = experts * block
    pieces = ((GROUPS, X - 1), (GROUPS, Y - 1))
    wide = max(X, Y) - 1
    return pl.pallas_call(
        functools.partial(step_kernel, sizes, cap),
        out_shape=(
            jax.ShapeDtypeStruct((tokens, mixer_out.shape[1]), bf16),
            jax.ShapeDtypeStruct((rows, share), bf16),
        ),
        in_specs=[vmem] * 11 + [hbm] * 4,
        out_specs=(vmem, vmem),
        scratch_shapes=[
            pltpu.VMEM((slots, tokens, 2 * width), bf16),
            pltpu.VMEM((2 * width, lanes), bf16),
            pltpu.VMEM((tokens, lanes), f32),
            pltpu.VMEM((tokens, lanes), f32),
            pltpu.VMEM((8, lanes), f32),
            pltpu.VMEM((8, lanes), f32),
            pltpu.VMEM((8, lanes), f32),
            pltpu.VMEM((16 + width, lanes), f32),
            pltpu.VMEM((experts, rows), f32),
            pltpu.VMEM((experts, rows), f32),
            pltpu.VMEM((experts, rows), f32),
            pltpu.VMEM((total, rows), bf16),
            pltpu.VMEM((total, rows), f32),
            pltpu.VMEM((rows, total), bf16),
            pltpu.VMEM((rows, total), bf16),
            pltpu.VMEM((total, half), bf16),
            pltpu.VMEM((Y, X, total, half), bf16),
            pltpu.VMEM((T * half, 4 * hidden), bf16),
            pltpu.VMEM((8, 128), f32),
            pltpu.VMEM((Y, X, total // 4, 2 * hidden), bf16),
            pltpu.VMEM((total, half), bf16),
            pltpu.VMEM((total, half), bf16),
            pltpu.VMEM((Y, X, tokens, columns), bf16),
            pltpu.VMEM(mixer_out.shape, bf16),
            pltpu.VMEM(gate.shape, bf16),
            pltpu.VMEM(up.shape, bf16),
            pltpu.VMEM(down.shape, bf16),
            dma((4,)),
            dma((slots,)),
            dma((slots,)),
            dma((experts,)),
            dma((experts,)),
            dma((experts,)),
            dma((experts,)),
        ]
        + [dma((GROUPS, wide))] * 4
        + [dma((2, wide))] * 8,
        compiler_params=pltpu.CompilerParams(
            collective_id=0, has_side_effects=True, vmem_limit_bytes=60 * 1024 * 1024
        ),
    )(
        query_input,
        key_input,
        value_input,
        cosine,
        sine,
        query_gain[:, None],
        key_gain[:, None],
        moe_input,
        moe_gain[None, :],
        routes.T,
        route_weight.T,
        mixer_out,
        gate,
        up,
        down,
    )


def solution(mesh, grid=None):
    n_ep, n_tp = mesh.shape["ep"], mesh.shape["tp"]
    sizes = grid or (n_ep // CORES, 4, n_tp // 4)
    Z, Y, X = sizes
    torus = Mesh(mesh.devices.reshape(Z, CORES, Y, X), AXES)
    ep, tp = ("z", "c"), ("y", "x")
    placed = (
        P(ep, tp),
        P(ep, tp),
        P(ep, tp),
        P(),
        P(),
        P(None, tp),
        P(ep, None),
        P(),
        P(ep, None),
        P(ep, None),
        P(ep, None, tp),
        P(ep, None, tp),
        P(ep, None, tp),
    )
    return jax.shard_map(
        functools.partial(on_device, sizes),
        mesh=torus,
        in_specs=placed,
        out_specs=(P(ep, tp), P(ep, tp)),
        check_vma=False,
    )
```

time: 328 us -> 190 us (0.58)
  waiting for transfers between devices: 150 us -> 0 us
  Pallas kernels: 35.5 us -> 173 us
  blocking collectives: 57.5 us -> 0 us
  local copies, waits for them, and re-layouts: 36.9 us -> 12.9 us
  starting transfers between devices: 15.2 us -> 0 us
  between operations: 14.1 us -> 0.67 us
  matrix products: 11 us -> 0 us
  other arithmetic: 7.26 us -> 0.99 us
    pallas_call x2 -> x1, Pallas kernels: 35.5 us -> 173 us  [on_device(): pl.pallas_call(functools.partial(step_kernel, sizes, cap), out_shape=(jax...]
    all_gather x3 -> x0, waiting for transfers between devices: 133 us -> none  [the longest x1 67.1 us: on_device(): incoming = lax.all_gather(received, TP, axis=3, tiled=True)]
    all_to_all x1 -> x0, blocking collectives: 44.4 us -> none  [on_device(): lax.all_to_all(own_columns[sources], 'ep', split_axis=0, concat_axis=0, t...]
    all_to_all x2 -> x0, waiting for transfers between devices: 16.2 us -> none  [the longest x1 16.2 us: on_device(): lax.all_to_all(expert_out, 'ep', split_axis=0, concat_axis=0, tiled=True)]
    all_to_all x2 -> x0, starting transfers between devices: 15 us -> none  [the longest x1 10.4 us: on_device(): lax.all_to_all(expert_out, 'ep', split_axis=0, concat_axis=0, tiled=True)]
    all_gather x1 -> x0, blocking collectives: 13.1 us -> none  [gather_axes(): x = lax.all_gather(x, axis, axis=dim, tiled=True)]
    dot_general x4 -> x0, matrix products: 11 us -> none  [the longest x1 4.72 us: on_device(): jnp.einsum('sjcd,jdf->sjcf', incoming, expert_gate, preferred_element_typ...]
    transpose x2 -> x0, local copies, waits for them, and re-layouts: 7.89 us -> none  [joined_along(): parts = jnp.moveaxis(parts, 0, dim)]
  transfers between devices with their start and end apart: 5 -> 0, of which waited for: 4 -> 0; matrix products, arithmetic and copies ran while one was open for 11% -> 0% of each run, Pallas kernels for 11% -> 0%
where the time goes in v2:
time: 190 us; the launch traced here: 188 us
  Pallas kernels  173 us (91%)
  local copies, waits for them, and re-layouts  12.9 us (7%)
    pallas_call x1, Pallas kernels, on_device(): pl.pallas_call(functools.partial(step_kernel, sizes, cap), out_shape=(jax...  173 us
    unnamed x8, local copies, waits for them, and re-layouts  10.1 us

profile of v2, /device:TPU:1, one launch (start us, length us, event | category | flops | bytes accessed | tf_op | source)
XLA Modules:
  0.0 187.9 jit_solution(10632472193206216567)
XLA Ops:
  0.6 0.0 copy-start
  0.7 1.4 copy.19.qg_ref
  2.1 1.4 copy.20.kg_ref
  3.4 0.1 broadcast_multiply_fusion.1
  3.5 0.9 fusion
  4.4 1.6 copy.17.k_ref
  6.0 1.6 copy.18.v_ref
  7.6 2.4 %copy.15 = bf16[1,4096,64]{2,1,0:T(8,128)(2,1)} copy(bf16[1,4096,64]{1,2,0:T(8,128)(2,1)} %param.23) | data formatting | bytes 1048576 | tf_op args[10]
  10.0 0.0 copy-done
  10.0 1.4 copy.16
  11.3 173.3 %shard_map.140 = (bf16[512,256]{1,0:T(8,128)(2,1)}, bf16[256,256]{1,0:T(8,128)(2,1)}) custom-call(bf16[512,128]{1,0:T(8,128)(2,1)} %q_ref.1, bf16[512,64]{1,0:T(8,128)(2,1)} %copy.17.k_ref, bf16[512,64]{1,0:T(8,128)(2,1)} %copy.18.v_ref, f32[32,512]{1,0:T(8,128)} %get-tuple-element.3.cos_ref, f32[32,512]{1,0:T(8,128)} %get-tuple-element.2.sin_ref, ...), custom_call_target="tpu_custom_call" | custom-call | tf_op jit(solution)/shard_map/pallas_call | solution.py:632
  184.7 1.7 copy.23
  186.3 1.6 copy.24
  (2 shorter events, 0.0 us)
Async XLA Ops:
  0.6 9.3 %copy-start = (bf16[1,4096,64]{1,2,0:T(8,128)(2,1)S(1)}, bf16[1,4096,64]{1,2,0:T(8,128)(2,1)}, u32[]{:S(2)}) copy-start(bf16[1,4096,64]{1,2,0:T(8,128)(2,1)} %param.24) | copy-start | bytes 1572868

commit v3 on v2

v3 whole, which is shorter than its diff:
```python
import functools

import jax
import jax.numpy as jnp
from jax import lax
from jax.experimental import pallas as pl
from jax.experimental.pallas import tpu as pltpu
from jax.sharding import Mesh
from jax.sharding import PartitionSpec as P

GRID_W = 64
TOP_K = 2
CORES = 2
AXES = ("z", "c", "y", "x")
epsilon = 1e-06
base_theta = 10000.0
log2e = 1.4426950408889634
MESH = pl.DeviceIdType.MESH


def rope_tables(positions, head_width):
    quarter = head_width // 4
    inverse = base_theta ** (-jnp.arange(quarter, dtype=jnp.float32) / quarter)
    grid_row = (positions // GRID_W).astype(jnp.float32)
    grid_col = (positions % GRID_W).astype(jnp.float32)
    angles = jnp.concatenate(
        [inverse[:, None] * grid_row[None, :], inverse[:, None] * grid_col[None, :]], axis=0
    )
    return (jnp.cos(angles), jnp.sin(angles))


def rotated(x, cosine, sine, gain):
    scale = lax.rsqrt(jnp.mean(x * x, axis=0, keepdims=True) + epsilon)
    x = x * scale * gain
    half = x.shape[0] // 2
    first, second = x[:half], x[half:]
    return jnp.concatenate(
        [first * cosine - second * sine, first * sine + second * cosine], axis=0
    )


def ring_offsets(size):
    offsets = [0]
    for step in range(1, size // 2 + 1):
        offsets.append(step)
        if step < size - step:
            offsets.append(-step)
    return offsets


def step_kernel(
    sizes,
    cap,
    q_hbm,
    k_hbm,
    v_hbm,
    cos_hbm,
    sin_hbm,
    qg_hbm,
    kg_hbm,
    x_hbm,
    xg_hbm,
    routes_hbm,
    share_hbm,
    mixer_hbm,
    gate_hbm,
    up_hbm,
    down_hbm,
    attn_hbm,
    moe_hbm,
    q_ref,
    k_ref,
    v_ref,
    cos_ref,
    sin_ref,
    qg_ref,
    kg_ref,
    x_ref,
    xg_ref,
    routes_ref,
    share_ref,
    mixer_ref,
    gate_ref,
    up_ref,
    down_ref,
    attn_ref,
    moe_ref,
    kv_ref,
    qt_ref,
    s0_ref,
    s1_ref,
    x0_ref,
    x1_ref,
    m_ref,
    o_ref,
    count_ref,
    weight_ref,
    pick_ref,
    combine_ref,
    chi_ref,
    clo_ref,
    disp_ref,
    rows_ref,
    gu_ref,
    hid_ref,
    eo_ref,
    back_ref,
    att_ref,
    load_sem,
    store_sem,
    kv_send,
    kv_recv,
    d_send,
    d_recv,
    r_send,
    r_recv,
    g_send,
    g_recv,
):
    Z, Y, X = sizes
    T = Y * X
    experts = Z * CORES
    z, c = lax.axis_index("z"), lax.axis_index("c")
    y, x = lax.axis_index("y"), lax.axis_index("x")
    ep = z * CORES + c
    tp = y * X + x
    offsets = ring_offsets(Z)
    places = [(rel, dc) for rel in offsets for dc in range(CORES)]
    block = 2 * cap
    f32, bf16 = jnp.float32, jnp.bfloat16

    def line(rel, dc):
        return {"z": lax.rem(z + (rel + Z), Z), "c": lax.rem(c + dc, CORES)}

    barrier = pltpu.get_barrier_semaphore()
    greeted = 0
    for rel, dc in reversed(places[1:]):
        pl.semaphore_signal(barrier, inc=1, device_id=line(rel, dc), device_id_type=MESH)
        greeted += 1
    for axis, at, size in (("x", x, X), ("y", y, Y)):
        for step in (1, size - 1) if size > 1 else ():
            device = {axis: lax.rem(at + step, size)}
            pl.semaphore_signal(barrier, inc=1, device_id=device, device_id_type=MESH)
            greeted += 1

    pairs = (
        (x_hbm, x_ref),
        (routes_hbm, routes_ref),
        (share_hbm, share_ref),
        (xg_hbm, xg_ref),
        (k_hbm, k_ref),
        (v_hbm, v_ref),
        (cos_hbm, cos_ref),
        (sin_hbm, sin_ref),
        (kg_hbm, kg_ref),
        (q_hbm, q_ref),
        (qg_hbm, qg_ref),
        (gate_hbm, gate_ref),
        (up_hbm, up_ref),
        (down_hbm, down_ref),
        (mixer_hbm, mixer_ref),
    )
    loads = [
        pltpu.make_async_copy(src, dst, load_sem.at[n]) for n, (src, dst) in enumerate(pairs)
    ]
    for load in loads:
        load.start()

    def remote(src, dst, send, recv, device):
        return pltpu.make_async_remote_copy(
            src_ref=src, dst_ref=dst, send_sem=send, recv_sem=recv, device_id=device, device_id_type=MESH
        )

    def column(row):
        return jnp.broadcast_to(row, (8, row.shape[1])).T[:, :1]

    rows, features = x_ref.shape
    share = features // T
    half = share // 2
    for load in loads[1:3]:
        load.wait()
    expert_at = lax.broadcasted_iota(jnp.int32, (experts, rows), 0)
    first = routes_ref[0:1, :] == expert_at
    second = routes_ref[1:2, :] == expert_at
    total_share = share_ref[0:1, :] + share_ref[1:2, :]
    named = jnp.where(first | second, 1.0, 0.0)
    earlier = jnp.where(
        lax.broadcasted_iota(jnp.int32, (rows, rows), 0)
        < lax.broadcasted_iota(jnp.int32, (rows, rows), 1),
        1.0,
        0.0,
    ).astype(bf16)
    count = jnp.dot(named.astype(bf16), earlier, preferred_element_type=f32)
    count_ref[...] = jnp.where(named > 0.0, count, -1.0)
    weight_ref[...] = jnp.where(first, share_ref[0:1, :] / total_share, 0.0) + jnp.where(
        second, share_ref[1:2, :] / total_share, 0.0
    )
    slot_at = lax.broadcasted_iota(jnp.int32, (block, rows), 0)
    slot_at = jnp.where(slot_at < cap, slot_at, slot_at - cap).astype(f32)

    @pl.loop(0, experts)
    def _(expert):
        here = count_ref[pl.ds(expert, 1), :] == slot_at
        at = pl.ds(pl.multiple_of(expert * block, block), block)
        pick_ref[at, :] = jnp.where(here, 1.0, 0.0).astype(bf16)
        combine_ref[at, :] = jnp.where(here, weight_ref[pl.ds(expert, 1), :], 0.0)

    loads[0].wait()
    loads[3].wait()
    chunk = 512
    squares = jnp.zeros((rows, 128), f32)
    for start in range(0, features, chunk):
        part = x_ref[:, start : start + chunk].astype(f32)
        part = part * part
        for lane in range(0, chunk, 128):
            squares = squares + part[:, lane : lane + 128]
    mean = jnp.sum(squares, axis=1, keepdims=True) * (1.0 / features)
    own = pl.ds(pl.multiple_of(tp * share, share), share)
    normed = (x_ref[:, own].astype(f32) * lax.rsqrt(mean + epsilon) * xg_ref[:, own]).astype(bf16)
    picked = jnp.dot(pick_ref[...], normed, preferred_element_type=f32)
    picked = picked.reshape(experts, block, share)
    picked = jnp.concatenate([picked[:, :cap, :half], picked[:, cap:, half:]], axis=1)
    disp_ref[...] = picked.reshape(experts * block, half).astype(bf16)

    for load in loads[4:]:
        load.wait()
    width = k_ref.shape[0]
    k_t = rotated(k_ref[...].astype(f32), cos_ref[...], sin_ref[...], column(kg_ref[...]))
    kv_ref[0] = jnp.concatenate([k_t, v_ref[...].astype(f32)], axis=0).T.astype(bf16)

    tokens = q_ref.shape[0]
    heads = q_ref.shape[1] // width
    lanes = heads * tokens
    q_t = q_ref[...].astype(f32).T
    q_gain = column(qg_ref[...])
    for head in range(heads):
        turned = rotated(
            q_t[head * width : (head + 1) * width], cos_ref[...], sin_ref[...], q_gain
        )
        turned = turned.astype(bf16).astype(f32) * (width ** (-0.5))
        qt_ref[:width, head * tokens : (head + 1) * tokens] = turned.astype(bf16)
    qt_ref[width:, :] = jnp.zeros((width, lanes), bf16)
    m_ref[...] = jnp.full(m_ref.shape, -1e30, f32)
    o_ref[...] = jnp.zeros(o_ref.shape, f32)

    hidden_width = gate_ref.shape[0]
    for t in range(T):
        top, low, to = t * share, t * share + half, t * half
        gu_ref[:, to : to + half] = jnp.concatenate(
            [
                gate_ref[:, top : top + half],
                up_ref[:, top : top + half],
                gate_ref[:, low : low + half],
                up_ref[:, low : low + half],
            ],
            axis=0,
        )
    for e in range(0, experts * block, 256):
        turned = combine_ref[e : e + 256, :].T
        high = turned.astype(bf16)
        chi_ref[:, e : e + 256] = high
        clo_ref[:, e : e + 256] = (turned - high.astype(f32)).astype(bf16)

    pl.semaphore_wait(barrier, greeted)

    def expert_rows(rel, dc):
        target = line(rel, dc)
        return pl.ds(pl.multiple_of((target["z"] * CORES + target["c"]) * block, block), block)

    def dispatch(p):
        rel, dc = places[p]
        return remote(
            disp_ref.at[expert_rows(-rel, dc)],
            rows_ref.at[y, x, pl.ds(p * block, block)],
            d_send.at[p],
            d_recv.at[p],
            line(-rel, dc),
        )

    kept = pltpu.make_async_copy(
        disp_ref.at[expert_rows(0, 0)], rows_ref.at[y, x, pl.ds(0, block)], d_recv.at[0]
    )
    kept.start()
    for p in range(1, len(places)):
        dispatch(p).start()

    def base(step):
        return 2 + 4 * (step - 1)

    last = Z // 2
    tail = base(last)

    def before(step):
        if isinstance(step, int):
            return 0 if step == 1 else base(step - 1)
        return lax.select(step == 1, 0, base(step - 1))

    def before_left(step):
        if isinstance(step, int):
            return 0 if step == 1 else base(step - 1) + 1
        return lax.select(step == 1, 0, base(step - 1) + 1)

    def moved(src, to, device):
        return remote(kv_ref.at[src], kv_ref.at[to], kv_send.at[to], kv_recv.at[to], device)

    def rightward(step):
        return moved(before(step), base(step), line(1, 0))

    def leftward(step):
        return moved(before_left(step), base(step) + 1, line(-1, 0))

    def across(src, to):
        return moved(src, to, line(0, 1))

    rightward(1).start()
    leftward(1).start()
    across(0, 1).start()
    s_ref, mx_ref = (s0_ref, s1_ref), (x0_ref, x1_ref)

    def scores(slot, buffer):
        s = jnp.dot(kv_ref[slot], qt_ref[...], preferred_element_type=f32)
        s_ref[buffer][...] = s
        mx_ref[buffer][...] = jnp.max(s.reshape(tokens // 8, 8, lanes), axis=0)

    def absorb(slot, buffer):
        old = m_ref[...]
        new = jnp.maximum(old, jnp.max(mx_ref[buffer][...], axis=0, keepdims=True) * log2e)
        m_ref[...] = new
        factor = jnp.exp2(old - new)
        p = jnp.exp2(s_ref[buffer][...] * log2e - new[:1]).astype(bf16)
        v_t = kv_ref[slot].T[width:]
        lhs = jnp.concatenate([jnp.ones((16, tokens), bf16), v_t], axis=0)
        part = jnp.dot(lhs, p, preferred_element_type=f32)
        o_ref[...] = o_ref[...] * factor[:1] + part

    def stage_copies(ref, begin, length, x_first, stage, n):
        moving_x = x_first == (stage < 2)
        at, size = (x, X) if moving_x else (y, Y)
        if size == 1:
            return []
        found = []
        for way, step in enumerate((1, -1)):
            behind = lax.rem(at - step + size, size)
            opposite = lax.rem(at + 2, size)
            device = {"x" if moving_x else "y": lax.rem(at + step + size, size)}
            if stage % 2 == 0:
                piece = pl.ds(begin, length)
                out_at, in_at = at, behind
            else:
                piece = pl.ds(begin + way * (length // 2), length // 2)
                out_at, in_at = behind, opposite
            every = pl.ds(0, Y if moving_x else X)

            def view(index):
                if stage < 2:
                    where = (y, index) if moving_x else (index, x)
                else:
                    where = (every, index) if moving_x else (index, every)
                return ref.at[where[0], where[1], piece]

            send, recv = g_send.at[n, stage, way], g_recv.at[n, stage, way]
            found.append((view(out_at), view(in_at), send, recv, device))
        return found

    def gather_stage(which, stage):
        ref, pieces, n = which
        found = []
        for number, (begin, length) in enumerate(pieces):
            found += stage_copies(ref, begin, length, number % 2 == 0, stage, n + number)
        return found

    def go(which, stage):
        for out, _, send, recv, device in gather_stage(which, stage):
            remote(out, out, send, recv, device).start()

    def come(which, stage):
        for _, into, send, recv, device in gather_stage(which, stage):
            remote(into, into, send, recv, device).wait_recv()

    def gone(which):
        for stage in range(4):
            for out, _, send, recv, device in gather_stage(which, stage):
                remote(out, out, send, recv, device).wait_send()

    def onward(which, stage):
        come(which, stage)
        go(which, stage + 1)

    groups = 4
    per_group = len(places) // groups
    span = per_group * block
    pack = per_group * cap // 2
    att_half = tokens // 2
    routed = [
        (rows_ref, [(g * span, span) for g in (2 * m, 2 * m + 1)], 2 * m) for m in range(2)
    ]
    hidden_units = [
        (hid_ref, [(g * pack, pack) for g in (2 * m, 2 * m + 1)], 4 + 2 * m) for m in range(2)
    ]
    attended_all = (att_ref, [(0, att_half), (att_half, att_half)], 8)

    def dispatched(m):
        for p in range(2 * m * per_group, 2 * (m + 1) * per_group):
            if p == 0:
                kept.wait()
            else:
                dispatch(p).wait_recv()
        go(routed[m], 0)

    def gate_up(m):
        for group in (2 * m, 2 * m + 1):
            at = pl.ds(group * span, span)
            total = None
            for t in range(0, T, min(T, 4)):
                many = range(t, min(t + 4, T))
                lhs = jnp.concatenate([rows_ref[u // X, u % X, at, :] for u in many], axis=1)
                term = lax.dot_general(
                    lhs,
                    gu_ref[:, t * half : (t + len(many)) * half],
                    (((1,), (1,)), ((), ())),
                    preferred_element_type=f32,
                )
                total = term if total is None else total + term
            both = total.reshape(per_group, block, 4 * hidden_width)
            both = both[:, :cap, : 2 * hidden_width] + both[:, cap:, 2 * hidden_width :]
            both = both.reshape(per_group * cap, 2 * hidden_width)
            gate = both[:, :hidden_width]
            up = both[:, hidden_width:]
            hidden = gate / (1.0 + jnp.exp(-gate)) * up
            hidden = jnp.concatenate([hidden[:pack], hidden[pack:]], axis=1)
            hid_ref[y, x, group * pack : (group + 1) * pack, :] = hidden.astype(bf16)
        go(hidden_units[m], 0)

    def giveback(p):
        rel, dc = places[p]
        mine = pl.ds(pl.multiple_of(ep * block, block), block)
        return remote(
            eo_ref.at[pl.ds(p * block, block)], back_ref.at[mine], r_send.at[p], r_recv.at[p], line(rel, dc)
        )

    def returned(p):
        rel, dc = places[p]
        at = expert_rows(-rel, dc)
        return remote(back_ref.at[at], back_ref.at[at], r_send.at[p], r_recv.at[p], line(rel, dc))

    own_back = pltpu.make_async_copy(
        eo_ref.at[pl.ds(0, block)],
        back_ref.at[pl.ds(pl.multiple_of(ep * block, block), block)],
        r_recv.at[0],
    )

    def down(m):
        for group in (2 * m, 2 * m + 1):
            at = slice(group * pack, (group + 1) * pack)
            lo = jnp.concatenate(
                [hid_ref[u // X, u % X, at, :hidden_width] for u in range(T)], axis=1
            )
            hi = jnp.concatenate(
                [hid_ref[u // X, u % X, at, hidden_width:] for u in range(T)], axis=1
            )
            out = jnp.dot(
                jnp.concatenate([lo, hi], axis=0), down_ref[...], preferred_element_type=f32
            )
            out = out.reshape(per_group, cap, share)
            out = jnp.concatenate([out[:, :, :half], out[:, :, half:]], axis=1)
            eo_ref[group * span : (group + 1) * span, :] = out.reshape(span, half).astype(bf16)
            for p in range(group * per_group, (group + 1) * per_group):
                if p == 0:
                    own_back.start()
                else:
                    giveback(p).start()

    def attended_out():
        attended = o_ref[16:, :] / o_ref[:1, :]
        for head in range(heads):
            piece = attended[:, head * tokens : (head + 1) * tokens].T
            att_ref[y, x, :, head * width : (head + 1) * width] = piece.astype(bf16)
        go(attended_all, 0)

    scores(0, 0)
    across(0, 1).wait_recv()
    scores(1, 1)
    absorb(0, 0)

    events = {
        0: [
            ("D0", lambda: dispatched(0)),
            ("G01", lambda: onward(routed[0], 0)),
            ("G02", lambda: onward(routed[0], 1)),
            ("G03", lambda: onward(routed[0], 2)),
            ("D1", lambda: dispatched(1)),
        ],
        2: [("G11", lambda: onward(routed[1], 0))],
        3: [
            ("G12", lambda: onward(routed[1], 1)),
            ("G04", lambda: come(routed[0], 3)),
            ("GU0", lambda: gate_up(0)),
        ],
        5: [("G13", lambda: onward(routed[1], 2)), ("H01", lambda: onward(hidden_units[0], 0))],
        6: [("H02", lambda: onward(hidden_units[0], 1))],
        7: [
            ("G14", lambda: come(routed[1], 3)),
            ("GU1", lambda: gate_up(1)),
            ("H03", lambda: onward(hidden_units[0], 2)),
        ],
        8: [
            ("H11", lambda: onward(hidden_units[1], 0)),
            ("H04", lambda: come(hidden_units[0], 3)),
            ("DN0", lambda: down(0)),
        ],
        9: [
            ("ATT", attended_out),
            ("H12", lambda: onward(hidden_units[1], 1)),
            ("A1", lambda: onward(attended_all, 0)),
            ("H13", lambda: onward(hidden_units[1], 2)),
            ("A2", lambda: onward(attended_all, 1)),
            ("H14", lambda: come(hidden_units[1], 3)),
            ("DN1", lambda: down(1)),
            ("A3", lambda: onward(attended_all, 2)),
            ("A4", lambda: come(attended_all, 3)),
        ],
    }

    def run(number):
        for name, event in events.get(number, ()):
            event()

    by_step = {}
    for number in sorted(events):
        by_step.setdefault(number if number in (0, 9) else min(max(number, 1), last), []).append(number)

    run(0)

    @pl.loop(1, last)
    def _(step):
        at = base(step)
        rightward(step).wait_recv()
        rightward(step + 1).start()
        across(at, at + 2).start()
        leftward(step).wait_recv()

        @pl.when(step < last - 1)
        def _():
            leftward(step + 1).start()

        across(at + 1, at + 3).start()
        for number in range(1, last):
            if number in by_step:

                @pl.when(step == number)
                def _(number=number):
                    for event in by_step[number]:
                        run(event)

        @pl.loop(0, 2)
        def _(pair):
            even = at + 2 * pair


            @pl.when(pair == 1)
            def _():
                across(at, at + 2).wait_recv()
                across(at + 1, at + 3).wait_recv()

            scores(even, 0)
            absorb(even - 1, 1)
            scores(even + 1, 1)
            absorb(even, 0)

    rightward(last).wait_recv()
    across(tail, tail + 1).start()
    for event in by_step.get(last, ()):
        run(event)
    scores(tail, 0)
    absorb(tail - 1, 1)
    across(tail, tail + 1).wait_recv()
    scores(tail + 1, 1)
    absorb(tail, 0)
    absorb(tail + 1, 1)
    run(9)

    lhs = jnp.concatenate([att_ref[u // X, u % X] for u in range(T)], axis=1)
    attn_ref[...] = jnp.dot(lhs, mixer_ref[...], preferred_element_type=f32).astype(bf16)
    attn_out = pltpu.make_async_copy(attn_ref, attn_hbm, store_sem.at[0])
    attn_out.start()

    own_back.wait()
    for p in range(1, len(places)):
        returned(p).wait_recv()
    back = back_ref[...].astype(f32).reshape(experts, block, half)
    blank = jnp.zeros((experts, cap, half), f32)
    wide = jnp.concatenate(
        [
            jnp.concatenate([back[:, :cap], blank], axis=1),
            jnp.concatenate([blank, back[:, cap:]], axis=1),
        ],
        axis=2,
    )
    wide = wide.reshape(experts * block, share).astype(bf16)
    moe = jnp.dot(chi_ref[...], wide, preferred_element_type=f32)
    moe = moe + jnp.dot(clo_ref[...], wide, preferred_element_type=f32)
    moe_ref[...] = moe.astype(bf16)
    moe_out = pltpu.make_async_copy(moe_ref, moe_hbm, store_sem.at[1])
    moe_out.start()

    across(0, 1).wait_send()
    for step in range(1, last + 1):
        rightward(step).wait_send()
        if step < last:
            leftward(step).wait_send()
            across(base(step), base(step) + 2).wait_send()
            across(base(step) + 1, base(step) + 3).wait_send()
    across(tail, tail + 1).wait_send()
    for p in range(1, len(places)):
        dispatch(p).wait_send()
        giveback(p).wait_send()
    for which in routed + hidden_units + [attended_all]:
        gone(which)
    attn_out.wait()
    moe_out.wait()


def on_device(
    sizes,
    query_input,
    key_input,
    value_input,
    query_gain,
    key_gain,
    mixer_out,
    moe_input,
    moe_gain,
    routes,
    route_weight,
    expert_gate,
    expert_up,
    expert_down,
):
    Z, Y, X = sizes
    T = Y * X
    experts = Z * CORES
    tokens, columns = query_input.shape
    width = query_gain.shape[0]
    lanes = tokens * (columns // width)
    ep = lax.axis_index("z") * CORES + lax.axis_index("c")
    positions = ep * tokens + jnp.arange(tokens, dtype=jnp.int32)
    cosine, sine = rope_tables(positions, width)
    rows, features = moe_input.shape
    share = features // T
    half = share // 2
    cap = 3 * rows * TOP_K // (2 * experts)
    block = 2 * cap
    hidden = expert_gate.shape[2]
    vmem, anywhere = pltpu.VMEM, pl.BlockSpec(memory_space=pl.ANY)
    bf16, f32 = jnp.bfloat16, jnp.float32
    dma = pltpu.SemaphoreType.DMA
    total = experts * block
    operands = (
        query_input,
        key_input.T,
        value_input.T,
        cosine,
        sine,
        query_gain[None, :],
        key_gain[None, :],
        moe_input,
        moe_gain[None, :],
        routes.T,
        route_weight.T,
        mixer_out,
        expert_gate[0].T,
        expert_up[0].T,
        expert_down[0],
    )
    outs = (
        jax.ShapeDtypeStruct((tokens, mixer_out.shape[1]), bf16),
        jax.ShapeDtypeStruct((rows, share), bf16),
    )
    return pl.pallas_call(
        functools.partial(step_kernel, sizes, cap),
        out_shape=outs,
        in_specs=[anywhere] * len(operands),
        out_specs=(anywhere, anywhere),
        scratch_shapes=[vmem(item.shape, item.dtype) for item in operands + outs]
        + [
            vmem((experts, tokens, 2 * width), bf16),
            vmem((2 * width, lanes), bf16),
            vmem((tokens, lanes), f32),
            vmem((tokens, lanes), f32),
            vmem((8, lanes), f32),
            vmem((8, lanes), f32),
            vmem((8, lanes), f32),
            vmem((16 + width, lanes), f32),
            vmem((experts, rows), f32),
            vmem((experts, rows), f32),
            vmem((total, rows), bf16),
            vmem((total, rows), f32),
            vmem((rows, total), bf16),
            vmem((rows, total), bf16),
            vmem((total, half), bf16),
            vmem((Y, X, total, half), bf16),
            vmem((4 * hidden, T * half), bf16),
            vmem((Y, X, total // 4, 2 * hidden), bf16),
            vmem((total, half), bf16),
            vmem((total, half), bf16),
            vmem((Y, X, tokens, columns), bf16),
            dma((len(operands),)),
            dma((len(outs),)),
        ]
        + [dma((experts,))] * 6
        + [dma((10, 4, 2))] * 2,
        compiler_params=pltpu.CompilerParams(
            collective_id=0, has_side_effects=True, vmem_limit_bytes=60 * 1024 * 1024
        ),
    )(*operands)


def solution(mesh, grid=None):
    n_ep, n_tp = mesh.shape["ep"], mesh.shape["tp"]
    sizes = grid or (n_ep // CORES, 4, n_tp // 4)
    Z, Y, X = sizes
    torus = Mesh(mesh.devices.reshape(Z, CORES, Y, X), AXES)
    ep, tp = ("z", "c"), ("y", "x")
    placed = (
        P(ep, tp),
        P(ep, tp),
        P(ep, tp),
        P(),
        P(),
        P(None, tp),
        P(ep, None),
        P(),
        P(ep, None),
        P(ep, None),
        P(ep, None, tp),
        P(ep, None, tp),
        P(ep, None, tp),
    )
    return jax.shard_map(
        functools.partial(on_device, sizes),
        mesh=torus,
        in_specs=placed,
        out_specs=(P(ep, tp), P(ep, tp)),
        check_vma=False,
    )
```

time: 190 us -> 121 us (0.64)
  Pallas kernels: 173 us -> 116 us
  local copies, waits for them, and re-layouts: 12.9 us -> 3.24 us
    pallas_call x1, Pallas kernels: 173 us -> 116 us  [on_device(): pl.pallas_call(functools.partial(step_kernel, sizes, cap), out_shape=outs...]
    unnamed x8 -> x2, local copies, waits for them, and re-layouts: 10.1 us -> 3.24 us
    broadcast_in_dim x2 -> x0, local copies, waits for them, and re-layouts: 2.77 us -> none  [the longest x1 1.41 us: on_device(): query_gain[:, None]]
where the time goes in v3:
time: 121 us
  Pallas kernels  116 us (96%)
  local copies, waits for them, and re-layouts  3.24 us (3%)
    pallas_call x1, Pallas kernels, on_device(): pl.pallas_call(functools.partial(step_kernel, sizes, cap), out_shape=outs...  116 us
    unnamed x2, local copies, waits for them, and re-layouts  3.24 us

profile of v3, /device:TPU:1, one launch (start us, length us, event | category | flops | bytes accessed | tf_op | source)
XLA Modules:
  0.0 120.8 jit_solution(1616012582504151029)
XLA Ops:
  0.7 0.1 broadcast_multiply_fusion.1
  0.7 0.9 fusion
  1.6 115.9 %shard_map.140 = (bf16[512,256]{1,0:T(8,128)(2,1)}, bf16[256,256]{1,0:T(8,128)(2,1)}) custom-call(bf16[512,128]{1,0:T(8,128)(2,1)} %q_hbm.1, bf16[64,512]{1,0:T(8,128)(2,1)} %bitcast.17, bf16[64,512]{1,0:T(8,128)(2,1)} %bitcast.18, f32[32,512]{1,0:T(8,128)} %get-tuple-element.3.cos_hbm, f32[32,512]{1,0:T(8,128)} %get-tuple-element.2.sin_hbm, ...), custom_call_target="tpu_custom_call" | custom-call | tf_op jit(solution)/shard_map/pallas_call | solution.py:679
  117.5 1.7 %copy.17 = bf16[512,256]{1,0:T(8,128)(2,1)} copy(bf16[512,256]{1,0:T(8,128)(2,1)} %get-tuple-element.10) | data formatting | bytes 524288
  119.2 1.6 %copy.18 = bf16[256,256]{1,0:T(8,128)(2,1)} copy(bf16[256,256]{1,0:T(8,128)(2,1)} %get-tuple-element.11) | data formatting | bytes 262144
  (2 shorter events, 0.0 us)

commit v4 on v3

--- a/solution.py
+++ b/solution.py
@@ -138,7 +138,7 @@
         pl.semaphore_signal(barrier, inc=1, device_id=line(rel, dc), device_id_type=MESH)
         greeted += 1
     for axis, at, size in (("x", x, X), ("y", y, Y)):
-        for step in (1, size - 1) if size > 1 else ():
+        for step in (1, size - 1):
             device = {axis: lax.rem(at + step, size)}
             pl.semaphore_signal(barrier, inc=1, device_id=device, device_id_type=MESH)
             greeted += 1
@@ -281,7 +281,8 @@
         disp_ref.at[expert_rows(0, 0)], rows_ref.at[y, x, pl.ds(0, block)], d_recv.at[0]
     )
     kept.start()
-    for p in range(1, len(places)):
+    near = len(places) // 2
+    for p in reversed(range(1, near)):
         dispatch(p).start()
 
     def base(step):
@@ -300,21 +301,29 @@
             return 0 if step == 1 else base(step - 1) + 1
         return lax.select(step == 1, 0, base(step - 1) + 1)
 
-    def moved(src, to, device):
-        return remote(kv_ref.at[src], kv_ref.at[to], kv_send.at[to], kv_recv.at[to], device)
-
-    def rightward(step):
-        return moved(before(step), base(step), line(1, 0))
-
-    def leftward(step):
-        return moved(before_left(step), base(step) + 1, line(-1, 0))
-
-    def across(src, to):
-        return moved(src, to, line(0, 1))
-
-    rightward(1).start()
-    leftward(1).start()
-    across(0, 1).start()
+    part_rows = kv_ref.shape[1] // 2
+
+    def moved(src, to, part, device):
+        at = pl.ds(part * part_rows, part_rows)
+        return remote(
+            kv_ref.at[src, at], kv_ref.at[to, at], kv_send.at[to, part], kv_recv.at[to, part], device
+        )
+
+    def rightward(step, part):
+        return moved(before(step), base(step), part, line(1, 0))
+
+    def leftward(step, part):
+        return moved(before_left(step), base(step) + 1, part, line(-1, 0))
+
+    def across(src, to, part):
+        return moved(src, to, part, line(0, 1))
+
+    for part in range(2):
+        rightward(1, part).start()
+        leftward(1, part).start()
+        across(0, 1, part).start()
+    for p in reversed(range(near, len(places))):
+        dispatch(p).start()
     s_ref, mx_ref = (s0_ref, s1_ref), (x0_ref, x1_ref)
 
     def scores(slot, buffer):
@@ -333,58 +342,78 @@
         part = jnp.dot(lhs, p, preferred_element_type=f32)
         o_ref[...] = o_ref[...] * factor[:1] + part
 
-    def stage_copies(ref, begin, length, x_first, stage, n):
-        moving_x = x_first == (stage < 2)
-        at, size = (x, X) if moving_x else (y, Y)
-        if size == 1:
-            return []
-        found = []
-        for way, step in enumerate((1, -1)):
-            behind = lax.rem(at - step + size, size)
-            opposite = lax.rem(at + 2, size)
-            device = {"x" if moving_x else "y": lax.rem(at + step + size, size)}
-            if stage % 2 == 0:
-                piece = pl.ds(begin, length)
-                out_at, in_at = at, behind
-            else:
-                piece = pl.ds(begin + way * (length // 2), length // 2)
-                out_at, in_at = behind, opposite
-            every = pl.ds(0, Y if moving_x else X)
-
-            def view(index):
-                if stage < 2:
-                    where = (y, index) if moving_x else (index, x)
-                else:
-                    where = (every, index) if moving_x else (index, every)
-                return ref.at[where[0], where[1], piece]
-
-            send, recv = g_send.at[n, stage, way], g_recv.at[n, stage, way]
-            found.append((view(out_at), view(in_at), send, recv, device))
-        return found
-
-    def gather_stage(which, stage):
+    def piece_copies(which, kind, j=0):
         ref, pieces, n = which
         found = []
         for number, (begin, length) in enumerate(pieces):
-            found += stage_copies(ref, begin, length, number % 2 == 0, stage, n + number)
+            x_first = number % 2 == 0
+            along_x = x_first == (kind in ("near", "far"))
+            at, size = (x, X) if along_x else (y, Y)
+            other = (x, X) if x_first else (y, Y)
+            fixed = lax.rem(other[0] + (0, 3, 2, 1)[j], other[1])
+            for way, step in enumerate((1, -1)):
+                behind = lax.rem(at - step + size, size)
+                device = {"x" if along_x else "y": lax.rem(at + step + size, size)}
+                if kind in ("near", "then"):
+                    rows_at = pl.ds(begin, length)
+                    out_at, in_at = at, behind
+                else:
+                    rows_at = pl.ds(begin + way * (length // 2), length // 2)
+                    out_at, in_at = behind, lax.rem(at + 2, size)
+
+                def view(index):
+                    if kind in ("near", "far"):
+                        where = (y, index) if along_x else (index, x)
+                    else:
+                        where = (fixed, index) if along_x else (index, fixed)
+                    return ref.at[where[0], where[1], rows_at]
+
+                sem = {"near": 0, "far": 2, "then": 4 + 2 * j, "last": 12 + 2 * j}[kind] + way
+                found.append(
+                    (view(out_at), view(in_at), g_send.at[n + number, sem], g_recv.at[n + number, sem], device)
+                )
         return found
 
-    def go(which, stage):
-        for out, _, send, recv, device in gather_stage(which, stage):
+    def go(which, kind, j=0):
+        for out, _, send, recv, device in piece_copies(which, kind, j):
             remote(out, out, send, recv, device).start()
 
-    def come(which, stage):
-        for _, into, send, recv, device in gather_stage(which, stage):
+    def come(which, kind, j=0):
+        for _, into, send, recv, device in piece_copies(which, kind, j):
             remote(into, into, send, recv, device).wait_recv()
 
     def gone(which):
-        for stage in range(4):
-            for out, _, send, recv, device in gather_stage(which, stage):
+        kinds = [("near", 0), ("far", 0)] + [(k, j) for k in ("then", "last") for j in range(4)]
+        for kind, j in kinds:
+            for out, _, send, recv, device in piece_copies(which, kind, j):
                 remote(out, out, send, recv, device).wait_send()
 
-    def onward(which, stage):
-        come(which, stage)
-        go(which, stage + 1)
+    def gather_step(which, number):
+        if number == 0:
+            go(which, "near")
+            go(which, "then", 0)
+        elif number == 1:
+            come(which, "near")
+            go(which, "far")
+            go(which, "then", 1)
+            go(which, "then", 3)
+        elif number == 2:
+            come(which, "then", 0)
+            go(which, "last", 0)
+        elif number == 3:
+            come(which, "far")
+            go(which, "then", 2)
+        elif number == 4:
+            come(which, "then", 1)
+            come(which, "then", 3)
+            go(which, "last", 1)
+            go(which, "last", 3)
+        elif number == 5:
+            come(which, "then", 2)
+            go(which, "last", 2)
+        else:
+            for j in range(4):
+                come(which, "last", j)
 
     groups = 4
     per_group = len(places) // groups
@@ -395,9 +424,9 @@
         (rows_ref, [(g * span, span) for g in (2 * m, 2 * m + 1)], 2 * m) for m in range(2)
     ]
     hidden_units = [
-        (hid_ref, [(g * pack, pack) for g in (2 * m, 2 * m + 1)], 4 + 2 * m) for m in range(2)
+        (hid_ref, [(g * pack, pack) for g in (2 * m, 2 * m + 1)], 6 + 2 * m) for m in range(2)
     ]
-    attended_all = (att_ref, [(0, att_half), (att_half, att_half)], 8)
+    attended_all = (att_ref, [(0, att_half), (att_half, att_half)], 4)
 
     def dispatched(m):
         for p in range(2 * m * per_group, 2 * (m + 1) * per_group):
@@ -405,7 +434,7 @@
                 kept.wait()
             else:
                 dispatch(p).wait_recv()
-        go(routed[m], 0)
+        gather_step(routed[m], 0)
 
     def gate_up(m):
         for group in (2 * m, 2 * m + 1):
@@ -429,7 +458,6 @@
             hidden = gate / (1.0 + jnp.exp(-gate)) * up
             hidden = jnp.concatenate([hidden[:pack], hidden[pack:]], axis=1)
             hid_ref[y, x, group * pack : (group + 1) * pack, :] = hidden.astype(bf16)
-        go(hidden_units[m], 0)
 
     def giveback(p):
         rel, dc = places[p]
@@ -450,7 +478,8 @@
     )
 
     def down(m):
-        for group in (2 * m, 2 * m + 1):
+        gather_step(hidden_units[m], 6)
+        for group in (2 * m + 1, 2 * m):
             at = slice(group * pack, (group + 1) * pack)
             lo = jnp.concatenate(
                 [hid_ref[u // X, u % X, at, :hidden_width] for u in range(T)], axis=1
@@ -464,7 +493,7 @@
             out = out.reshape(per_group, cap, share)
             out = jnp.concatenate([out[:, :, :half], out[:, :, half:]], axis=1)
             eo_ref[group * span : (group + 1) * span, :] = out.reshape(span, half).astype(bf16)
-            for p in range(group * per_group, (group + 1) * per_group):
+            for p in reversed(range(group * per_group, (group + 1) * per_group)):
                 if p == 0:
                     own_back.start()
                 else:
@@ -475,109 +504,123 @@
         for head in range(heads):
             piece = attended[:, head * tokens : (head + 1) * tokens].T
             att_ref[y, x, :, head * width : (head + 1) * width] = piece.astype(bf16)
-        go(attended_all, 0)
+        gather_step(attended_all, 0)
 
     scores(0, 0)
-    across(0, 1).wait_recv()
+    for part in range(2):
+        across(0, 1, part).wait_recv()
     scores(1, 1)
     absorb(0, 0)
 
+    def gather_event(which, number):
+        return lambda: gather_step(which, number)
+
+    def last_gate_up(m):
+        gather_step(routed[m], 6)
+        gate_up(m)
+        gather_step(hidden_units[m], 0)
+
+    def at_hidden(m, number):
+        return (f"H{m}{number}", gather_event(hidden_units[m], number))
+
+    def at_routed(m, number):
+        return (f"G{m}{number}", gather_event(routed[m], number))
+
+    def at_attended(number):
+        return (f"A{number}", gather_event(attended_all, number))
+
     events = {
-        0: [
-            ("D0", lambda: dispatched(0)),
-            ("G01", lambda: onward(routed[0], 0)),
-            ("G02", lambda: onward(routed[0], 1)),
-            ("G03", lambda: onward(routed[0], 2)),
-            ("D1", lambda: dispatched(1)),
-        ],
-        2: [("G11", lambda: onward(routed[1], 0))],
-        3: [
-            ("G12", lambda: onward(routed[1], 1)),
-            ("G04", lambda: come(routed[0], 3)),
-            ("GU0", lambda: gate_up(0)),
-        ],
-        5: [("G13", lambda: onward(routed[1], 2)), ("H01", lambda: onward(hidden_units[0], 0))],
-        6: [("H02", lambda: onward(hidden_units[0], 1))],
-        7: [
-            ("G14", lambda: come(routed[1], 3)),
-            ("GU1", lambda: gate_up(1)),
-            ("H03", lambda: onward(hidden_units[0], 2)),
-        ],
-        8: [
-            ("H11", lambda: onward(hidden_units[1], 0)),
-            ("H04", lambda: come(hidden_units[0], 3)),
-            ("DN0", lambda: down(0)),
-        ],
-        9: [
+        (0, 1): [("D0", lambda: dispatched(0))],
+        (1, 1): [at_routed(0, n) for n in range(1, 5)],
+        (2, 0): [at_routed(0, 5), ("D1", lambda: dispatched(1))],
+        (3, 1): [("GU0", lambda: last_gate_up(0))],
+        (4, 0): [at_routed(1, 1)],
+        (4, 1): [at_hidden(0, 1), at_routed(1, 2)],
+        (5, 0): [at_routed(1, 3), at_hidden(0, 2)],
+        (5, 1): [at_hidden(0, 3)],
+        (6, 0): [at_routed(1, 4), at_hidden(0, 4)],
+        (6, 1): [at_routed(1, 5), at_hidden(0, 5)],
+        (7, 1): [("GU1", lambda: last_gate_up(1)), ("DN0", lambda: down(0))],
+        (8, 0): [at_hidden(1, 1)],
+        (8, 1): [at_hidden(1, 2), at_hidden(1, 3)],
+        (9, 1): [
+            at_hidden(1, 5),
             ("ATT", attended_out),
-            ("H12", lambda: onward(hidden_units[1], 1)),
-            ("A1", lambda: onward(attended_all, 0)),
-            ("H13", lambda: onward(hidden_units[1], 2)),
-            ("A2", lambda: onward(attended_all, 1)),
-            ("H14", lambda: come(hidden_units[1], 3)),
             ("DN1", lambda: down(1)),
-            ("A3", lambda: onward(attended_all, 2)),
-            ("A4", lambda: come(attended_all, 3)),
-        ],
+        ]
+        + [at_attended(n) for n in range(1, 7)],
+        (8, 2): [at_hidden(1, 4)],
     }
 
     def run(number):
         for name, event in events.get(number, ()):
             event()
 
-    by_step = {}
-    for number in sorted(events):
-        by_step.setdefault(number if number in (0, 9) else min(max(number, 1), last), []).append(number)
-
-    run(0)
+    run((0, 1))
 
     @pl.loop(1, last)
     def _(step):
         at = base(step)
-        rightward(step).wait_recv()
-        rightward(step + 1).start()
-        across(at, at + 2).start()
-        leftward(step).wait_recv()
-
-        @pl.when(step < last - 1)
+        for part in range(2):
+            rightward(step, part).wait_recv()
+            rightward(step + 1, part).start()
+            across(at, at + 2, part).start()
+            leftward(step, part).wait_recv()
+
+            @pl.when(step < last - 1)
+            def _(part=part):
+                leftward(step + 1, part).start()
+
+            across(at + 1, at + 3, part).start()
+            for number in range(1, last):
+                if (number, part) in events:
+
+                    @pl.when(step == number)
+                    def _(number=number, part=part):
+                        run((number, part))
+
+            @pl.when(step > 1)
+            def _(part=part):
+                even = at - 4 + 2 * part
+                if part == 1:
+                    for other in range(2):
+                        across(at - 4, at - 2, other).wait_recv()
+                        across(at - 3, at - 1, other).wait_recv()
+                scores(even, 0)
+                absorb(even - 1, 1)
+                scores(even + 1, 1)
+                absorb(even, 0)
+
+    for part in range(2):
+        rightward(last, part).wait_recv()
+        across(tail, tail + 1, part).start()
+    run((8, 0))
+
+    @pl.loop(0, 2)
+    def _(pair):
+        even = tail - 4 + 2 * pair
+
+        @pl.when(pair == 1)
         def _():
-            leftward(step + 1).start()
-
-        across(at + 1, at + 3).start()
-        for number in range(1, last):
-            if number in by_step:
-
-                @pl.when(step == number)
-                def _(number=number):
-                    for event in by_step[number]:
-                        run(event)
-
-        @pl.loop(0, 2)
-        def _(pair):
-            even = at + 2 * pair
-
-
-            @pl.when(pair == 1)
-            def _():
-                across(at, at + 2).wait_recv()
-                across(at + 1, at + 3).wait_recv()
-
-            scores(even, 0)
-            absorb(even - 1, 1)
-            scores(even + 1, 1)
-            absorb(even, 0)
-
-    rightward(last).wait_recv()
-    across(tail, tail + 1).start()
-    for event in by_step.get(last, ()):
-        run(event)
+            for part in range(2):
+                across(tail - 4, tail - 2, part).wait_recv()
+                across(tail - 3, tail - 1, part).wait_recv()
+
+        scores(even, 0)
+        absorb(even - 1, 1)
+        scores(even + 1, 1)
+        absorb(even, 0)
+
+    run((8, 1))
     scores(tail, 0)
     absorb(tail - 1, 1)
-    across(tail, tail + 1).wait_recv()
+    run((8, 2))
+    for part in range(2):
+        across(tail, tail + 1, part).wait_recv()
     scores(tail + 1, 1)
     absorb(tail, 0)
     absorb(tail + 1, 1)
-    run(9)
+    run((9, 1))
 
     lhs = jnp.concatenate([att_ref[u // X, u % X] for u in range(T)], axis=1)
     attn_ref[...] = jnp.dot(lhs, mixer_ref[...], preferred_element_type=f32).astype(bf16)
@@ -603,14 +646,15 @@
     moe_out = pltpu.make_async_copy(moe_ref, moe_hbm, store_sem.at[1])
     moe_out.start()
 
-    across(0, 1).wait_send()
-    for step in range(1, last + 1):
-        rightward(step).wait_send()
-        if step < last:
-            leftward(step).wait_send()
-            across(base(step), base(step) + 2).wait_send()
-            across(base(step) + 1, base(step) + 3).wait_send()
-    across(tail, tail + 1).wait_send()
+    for part in range(2):
+        across(0, 1, part).wait_send()
+        for step in range(1, last + 1):
+            rightward(step, part).wait_send()
+            if step < last:
+                leftward(step, part).wait_send()
+                across(base(step), base(step) + 2, part).wait_send()
+                across(base(step) + 1, base(step) + 3, part).wait_send()
+        across(tail, tail + 1, part).wait_send()
     for p in range(1, len(places)):
         dispatch(p).wait_send()
         giveback(p).wait_send()
@@ -618,6 +662,20 @@
         gone(which)
     attn_out.wait()
     moe_out.wait()
+
+
+def hand_over_kernel(a_in, b_in, a_out, b_out, a_ref, b_ref, sem):
+    moves = [
+        (pltpu.make_async_copy(src, ref, sem.at[n]), pltpu.make_async_copy(ref, dst, sem.at[n + 2]))
+        for n, (src, ref, dst) in enumerate(((a_in, a_ref, a_out), (b_in, b_ref, b_out)))
+    ]
+    for into, _ in moves:
+        into.start()
+    for into, out in moves:
+        into.wait()
+        out.start()
+    for _, out in moves:
+        out.wait()
 
 
 def on_device(
@@ -676,7 +734,7 @@
         jax.ShapeDtypeStruct((tokens, mixer_out.shape[1]), bf16),
         jax.ShapeDtypeStruct((rows, share), bf16),
     )
-    return pl.pallas_call(
+    results = pl.pallas_call(
         functools.partial(step_kernel, sizes, cap),
         out_shape=outs,
         in_specs=[anywhere] * len(operands),
@@ -707,12 +765,20 @@
             dma((len(operands),)),
             dma((len(outs),)),
         ]
-        + [dma((experts,))] * 6
-        + [dma((10, 4, 2))] * 2,
+        + [dma((experts, 2))] * 2
+        + [dma((experts,))] * 4
+        + [dma((10, 20))] * 2,
         compiler_params=pltpu.CompilerParams(
             collective_id=0, has_side_effects=True, vmem_limit_bytes=60 * 1024 * 1024
         ),
     )(*operands)
+    return pl.pallas_call(
+        hand_over_kernel,
+        out_shape=outs,
+        in_specs=[anywhere] * 2,
+        out_specs=(anywhere, anywhere),
+        scratch_shapes=[vmem(item.shape, item.dtype) for item in outs] + [dma((4,))],
+    )(*results)
 
 
 def solution(mesh, grid=None):

time: 121 us -> 105 us (0.87)
  Pallas kernels: 116 us -> 103 us
  local copies, waits for them, and re-layouts: 3.24 us -> 0 us
    pallas_call x1, Pallas kernels: 116 us -> 101 us  [on_device(): pl.pallas_call(functools.partial(step_kernel, sizes, cap), out_shape=outs...]
    unnamed x2 -> x0, local copies, waits for them, and re-layouts: 3.24 us -> none
    pallas_call x0 -> x1, Pallas kernels: none -> 1.73 us  [on_device(): pl.pallas_call(hand_over_kernel, out_shape=outs, in_specs=[anywhere] * 2,...]
where the time goes in v4:
time: 105 us; the launch traced here: 104 us
  Pallas kernels  103 us (98%)
    pallas_call x1, Pallas kernels, on_device(): pl.pallas_call(functools.partial(step_kernel, sizes, cap), out_shape=outs...  101 us

profile of v4, /device:TPU:1, one launch (start us, length us, event | category | flops | bytes accessed | tf_op | source)
XLA Modules:
  0.0 104.4 jit_solution(7404244908793239134)
XLA Ops:
  0.7 0.1 broadcast_multiply_fusion.1
  0.7 0.9 fusion
  1.6 100.8 %shard_map.140 = (bf16[512,256]{1,0:T(8,128)(2,1)}, bf16[256,256]{1,0:T(8,128)(2,1)}) custom-call(bf16[512,128]{1,0:T(8,128)(2,1)} %q_hbm.1, bf16[64,512]{1,0:T(8,128)(2,1)} %bitcast.17, bf16[64,512]{1,0:T(8,128)(2,1)} %bitcast.18, f32[32,512]{1,0:T(8,128)} %get-tuple-element.7.cos_hbm, f32[32,512]{1,0:T(8,128)} %get-tuple-element.6.sin_hbm, ...), custom_call_target="tpu_custom_call" | custom-call | tf_op jit(solution)/shard_map/pallas_call | solution.py:737
  102.5 1.7 %shard_map.141 = (bf16[512,256]{1,0:T(8,128)(2,1)}, bf16[256,256]{1,0:T(8,128)(2,1)}) custom-call(bf16[512,256]{1,0:T(8,128)(2,1)} %get-tuple-element.4.a_in, bf16[256,256]{1,0:T(8,128)(2,1)} %get-tuple-element.5.b_in), custom_call_target="tpu_custom_call" | custom-call | tf_op jit(solution)/shard_map/pallas_call | solution.py:775
  (2 shorter events, 0.0 us)

commit v5 on v4

--- a/solution.py
+++ b/solution.py
@@ -116,6 +116,7 @@
     r_recv,
     g_send,
     g_recv,
+    own_sem,
 ):
     Z, Y, X = sizes
     T = Y * X
@@ -272,13 +273,13 @@
         return remote(
             disp_ref.at[expert_rows(-rel, dc)],
             rows_ref.at[y, x, pl.ds(p * block, block)],
-            d_send.at[p],
-            d_recv.at[p],
+            d_send.at[0],
+            d_recv.at[0 if p < len(places) // 2 else 1],
             line(-rel, dc),
         )
 
     kept = pltpu.make_async_copy(
-        disp_ref.at[expert_rows(0, 0)], rows_ref.at[y, x, pl.ds(0, block)], d_recv.at[0]
+        disp_ref.at[expert_rows(0, 0)], rows_ref.at[y, x, pl.ds(0, block)], own_sem.at[0]
     )
     kept.start()
     near = len(places) // 2
@@ -306,7 +307,7 @@
     def moved(src, to, part, device):
         at = pl.ds(part * part_rows, part_rows)
         return remote(
-            kv_ref.at[src, at], kv_ref.at[to, at], kv_send.at[to, part], kv_recv.at[to, part], device
+            kv_ref.at[src, at], kv_ref.at[to, at], kv_send.at[0], kv_recv.at[to, part], device
         )
 
     def rightward(step, part):
@@ -370,7 +371,7 @@
 
                 sem = {"near": 0, "far": 2, "then": 4 + 2 * j, "last": 12 + 2 * j}[kind] + way
                 found.append(
-                    (view(out_at), view(in_at), g_send.at[n + number, sem], g_recv.at[n + number, sem], device)
+                    (view(out_at), view(in_at), g_send.at[(n + number) // 2], g_recv.at[n + number, sem], device)
                 )
         return found
 
@@ -383,10 +384,11 @@
             remote(into, into, send, recv, device).wait_recv()
 
     def gone(which):
-        kinds = [("near", 0), ("far", 0)] + [(k, j) for k in ("then", "last") for j in range(4)]
-        for kind, j in kinds:
-            for out, _, send, recv, device in piece_copies(which, kind, j):
-                remote(out, out, send, recv, device).wait_send()
+        ref, pieces, n = which
+        rows_sent = 15 * len(pieces) * pieces[0][1]
+        cells = 12 if rows_sent // 12 <= ref.shape[2] else 16
+        view = ref.at[:, pl.ds(0, cells // Y), pl.ds(0, rows_sent // cells)]
+        remote(view, view, g_send.at[n // 2], g_recv.at[0, 0], line(0, 1)).wait_send()
 
     def gather_step(which, number):
         if number == 0:
@@ -429,11 +431,11 @@
     attended_all = (att_ref, [(0, att_half), (att_half, att_half)], 4)
 
     def dispatched(m):
-        for p in range(2 * m * per_group, 2 * (m + 1) * per_group):
-            if p == 0:
-                kept.wait()
-            else:
-                dispatch(p).wait_recv()
+        if m == 0:
+            kept.wait()
+        begin = max(1, m * near) * block
+        here = rows_ref.at[y, x, pl.ds(begin, (m + 1) * near * block - begin)]
+        remote(here, here, d_send.at[0], d_recv.at[m], line(0, 1)).wait_recv()
         gather_step(routed[m], 0)
 
     def gate_up(m):
@@ -463,18 +465,13 @@
         rel, dc = places[p]
         mine = pl.ds(pl.multiple_of(ep * block, block), block)
         return remote(
-            eo_ref.at[pl.ds(p * block, block)], back_ref.at[mine], r_send.at[p], r_recv.at[p], line(rel, dc)
+            eo_ref.at[pl.ds(p * block, block)], back_ref.at[mine], r_send.at[0], r_recv.at[0], line(rel, dc)
         )
-
-    def returned(p):
-        rel, dc = places[p]
-        at = expert_rows(-rel, dc)
-        return remote(back_ref.at[at], back_ref.at[at], r_send.at[p], r_recv.at[p], line(rel, dc))
 
     own_back = pltpu.make_async_copy(
         eo_ref.at[pl.ds(0, block)],
         back_ref.at[pl.ds(pl.multiple_of(ep * block, block), block)],
-        r_recv.at[0],
+        own_sem.at[1],
     )
 
     def down(m):
@@ -628,8 +625,10 @@
     attn_out.start()
 
     own_back.wait()
-    for p in range(1, len(places)):
-        returned(p).wait_recv()
+    others = pl.ds(0, (len(places) - 1) * block)
+    remote(
+        back_ref.at[others], back_ref.at[others], r_send.at[0], r_recv.at[0], line(0, 1)
+    ).wait_recv()
     back = back_ref[...].astype(f32).reshape(experts, block, half)
     blank = jnp.zeros((experts, cap, half), f32)
     wide = jnp.concatenate(
@@ -646,18 +645,13 @@
     moe_out = pltpu.make_async_copy(moe_ref, moe_hbm, store_sem.at[1])
     moe_out.start()
 
-    for part in range(2):
-        across(0, 1, part).wait_send()
-        for step in range(1, last + 1):
-            rightward(step, part).wait_send()
-            if step < last:
-                leftward(step, part).wait_send()
-                across(base(step), base(step) + 2, part).wait_send()
-                across(base(step) + 1, base(step) + 3, part).wait_send()
-        across(tail, tail + 1, part).wait_send()
-    for p in range(1, len(places)):
-        dispatch(p).wait_send()
-        giveback(p).wait_send()
+    chunks = pl.ds(0, kv_ref.shape[0] - 1)
+    for ref, at, send, recv in (
+        (kv_ref, chunks, kv_send.at[0], kv_recv.at[0, 0]),
+        (disp_ref, others, d_send.at[0], d_recv.at[0]),
+        (eo_ref, others, r_send.at[0], r_recv.at[0]),
+    ):
+        remote(ref.at[at], ref.at[at], send, recv, line(0, 1)).wait_send()
     for which in routed + hidden_units + [attended_all]:
         gone(which)
     attn_out.wait()
@@ -765,9 +759,8 @@
             dma((len(operands),)),
             dma((len(outs),)),
         ]
-        + [dma((experts, 2))] * 2
-        + [dma((experts,))] * 4
-        + [dma((10, 20))] * 2,
+        + [dma((1,)), dma((experts, 2)), dma((1,)), dma((2,)), dma((1,)), dma((1,))]
+        + [dma((5,)), dma((10, 20)), dma((2,))],
         compiler_params=pltpu.CompilerParams(
             collective_id=0, has_side_effects=True, vmem_limit_bytes=60 * 1024 * 1024
         ),

time: 105 us -> 102 us (0.971)
  Pallas kernels: 103 us -> 98.7 us
    pallas_call x1, Pallas kernels: 101 us -> 96.9 us  [on_device(): pl.pallas_call(functools.partial(step_kernel, sizes, cap), out_shape=outs...]
where the time goes in v5:
time: 102 us; the launch traced here: 100 us
  Pallas kernels  98.7 us (97%)
    pallas_call x1, Pallas kernels, on_device(): pl.pallas_call(functools.partial(step_kernel, sizes, cap), out_shape=outs...  96.9 us

profile of v5, /device:TPU:1, one launch (start us, length us, event | category | flops | bytes accessed | tf_op | source)
XLA Modules:
  0.0 100.5 jit_solution(3215822743675113171)
XLA Ops:
  0.7 0.1 broadcast_multiply_fusion.1
  0.7 0.9 fusion
  1.6 96.9 %shard_map.140 = (bf16[512,256]{1,0:T(8,128)(2,1)}, bf16[256,256]{1,0:T(8,128)(2,1)}) custom-call(bf16[512,128]{1,0:T(8,128)(2,1)} %q_hbm.1, bf16[64,512]{1,0:T(8,128)(2,1)} %bitcast.17, bf16[64,512]{1,0:T(8,128)(2,1)} %bitcast.18, f32[32,512]{1,0:T(8,128)} %get-tuple-element.7.cos_hbm, f32[32,512]{1,0:T(8,128)} %get-tuple-element.6.sin_hbm, ...), custom_call_target="tpu_custom_call" | custom-call | tf_op jit(solution)/shard_map/pallas_call | solution.py:731
  98.6 1.7 %shard_map.141 = (bf16[512,256]{1,0:T(8,128)(2,1)}, bf16[256,256]{1,0:T(8,128)(2,1)}) custom-call(bf16[512,256]{1,0:T(8,128)(2,1)} %get-tuple-element.4.a_in, bf16[256,256]{1,0:T(8,128)(2,1)} %get-tuple-element.5.b_in), custom_call_target="tpu_custom_call" | custom-call | tf_op jit(solution)/shard_map/pallas_call | solution.py:768
  (2 shorter events, 0.0 us)
